TPU v7x, 128 devices: a whole 4x4x4 slice. The times are simulated.
128 devices in a mesh: fs: 32 (over z, y, core), tp: 4 (over x).
Axes of the slice: x: 4, y: 4, z: 4, core: 2. Of those that a mesh axis runs over, the one named last changes fastest.
Arguments:
- hidden_states: bfloat16 [2048, 2048], P('tp', 'fs'), may hold values from -6 to 6
- norm_gain: float32 [2048], P('fs'), may hold values from 0.1 to 1.9
- gate_master: float32 [8, 2048, 7168], P(None, 'fs', 'tp'), may hold values from -0.125 to 0.125
- up_master: float32 [8, 2048, 7168], P(None, 'fs', 'tp'), may hold values from -0.125 to 0.125
- down_master: float32 [8, 2048, 7168], P(None, 'fs', 'tp'), may hold values from -0.0625 to 0.0625
- expert_ids: int32 [2048, 2], P('tp'), may hold values from 0 to 7, all different within a row; in each aligned block of 512 rows (0 to 511, 512 to 1023, ...) at most 256 rows name the same one
- route_logits: float32 [2048, 2], P('tp'), may hold values from -6 to 6
Outputs:
- gate_serve: bfloat16 [8, 2048, 7168], P('tp', None, 'fs')
- up_serve: bfloat16 [8, 2048, 7168], P('tp', None, 'fs')
- down_serve: bfloat16 [8, 2048, 7168], P('tp', None, 'fs')
- combined: bfloat16 [2048, 2048], P('tp', 'fs')
Inputs may be any that keep to these rules, and one draw needn't show every extreme that they name: `expert_ids`: the 2 entries of a row differ. Among the rows of one index of tp (aligned blocks of 512 rows) no expert is named more than 256 times, and in some blocks one expert is named exactly 256 times.
All inputs are finite; a program needn't handle non-finite values.
Results may differ from a plain program's by a relative error of at most 0.018.
Values may be sent and summed in bfloat16 or wider, within the bound.
A program may use at most 128 MiB of HBM per device.

v0:
```python
import jax
import jax.numpy as jnp
from jax import lax
from jax.sharding import Mesh
from jax.sharding import PartitionSpec as P

FS = ("fs_0", "fs_1", "fs_2")


EPSILON = 1e-06


def side_by_side(arrays, axis, split_dim, concat_dim, along):
    ends, at = ([], 0)
    for a in arrays[:-1]:
        at += a.shape[along]
        ends.append(at)
    both = jnp.concatenate(arrays, axis=along)
    return tuple(
        jnp.split(
            lax.all_to_all(both, axis, split_axis=split_dim, concat_axis=concat_dim, tiled=True),
            ends,
            axis=along,
        )
    )


def from_everyone(shard, axis):
    length = lax.axis_size(axis)
    return lax.all_to_all(
        jnp.broadcast_to(shard[None], (length, *shard.shape)), axis, 0, 0, tiled=True
    )


def taken_together(shard, axis):
    return from_everyone(shard, axis).sum(axis=0)


def split_up(shard, dim, length):
    shape = shard.shape
    tiles = shard.reshape(*shape[:dim], length, shape[dim] // length, *shape[dim + 1 :])
    return jnp.moveaxis(tiles, dim, 0)


def sum_by_chip_2(shard, chips, core, dim):
    sizes = (lax.axis_size(chips), lax.axis_size(core))
    tiles = split_up(shard, dim, sizes[0] * sizes[1])
    inside = tiles.shape[1:]
    tiles = tiles.reshape(*sizes, *inside).swapaxes(0, 1).reshape(-1, *inside)
    tiles = lax.psum_scatter(tiles, core, scatter_dimension=0, tiled=True)
    return lax.psum_scatter(tiles, chips, scatter_dimension=0, tiled=True)[0]


def arrange(weights, groups, row_groups):
    experts, rows, columns = weights.shape
    blocks = row_groups // groups
    split = weights.reshape(experts // groups, groups, rows, blocks, columns // blocks)
    split = split.reshape(groups, experts // groups, rows, blocks, columns // blocks)
    return jnp.transpose(split, (0, 3, 1, 2, 4))


def regroup(moved, row_groups):
    return moved.reshape((row_groups,) + moved.shape[2:])


def settle(arrived):
    return arrived.reshape(arrived.shape[1], arrived.shape[2], arrived.shape[3])


def per_device(
    hidden_states, norm_gain, gate_master, up_master, down_master, expert_ids, route_logits
):
    groups = lax.axis_size("tp")
    row_groups = lax.axis_size(FS)
    experts = gate_master.shape[0]
    local_count = experts // groups
    tokens = hidden_states.shape[0]
    pieces = hidden_states.shape[1]
    model_width = pieces * row_groups
    capacity = tokens // 2
    scaled = norm_gain[None, :, None]
    gate_cast = arrange((scaled * gate_master).astype(jnp.bfloat16), groups, row_groups)
    up_cast = arrange((scaled * up_master).astype(jnp.bfloat16), groups, row_groups)
    down_cast = arrange(down_master.astype(jnp.bfloat16), groups, row_groups)
    sectioned = side_by_side((gate_cast, up_cast, down_cast), "tp", 0, 0, 1)
    landed = side_by_side(
        (
            regroup(sectioned[0], row_groups),
            regroup(sectioned[1], row_groups),
            regroup(sectioned[2], row_groups),
        ),
        FS,
        0,
        2,
        1,
    )
    gate_serve, up_serve, down_serve = (settle(landed[0]), settle(landed[1]), settle(landed[2]))
    values = hidden_states.astype(jnp.float32)
    squares = taken_together(jnp.sum(values * values, axis=1), FS)
    normed = (values * lax.rsqrt(squares / model_width + EPSILON)[:, None]).astype(jnp.bfloat16)
    weights = jax.nn.softmax(route_logits, axis=1)
    chosen = (expert_ids[:, :, None] == jnp.arange(experts, dtype=jnp.int32)[None, None, :]).astype(
        jnp.int32
    )
    chosen = chosen.reshape(tokens * 2, experts)
    before = jnp.cumsum(chosen, axis=0) - chosen
    position = jnp.sum(before * chosen, axis=1)
    slot_ids = expert_ids.reshape(-1) * capacity + position
    slot_table = (
        slot_ids[None, :] == jnp.arange(experts * capacity, dtype=jnp.int32)[:, None]
    ).astype(jnp.bfloat16)
    dispatch = jnp.sum(slot_table.reshape(experts * capacity, tokens, 2), axis=2)
    packed = jnp.dot(dispatch, normed, preferred_element_type=jnp.float32).astype(jnp.bfloat16)
    moved_rows = lax.all_to_all(
        packed.reshape(groups, local_count * capacity, pieces),
        "tp",
        split_axis=0,
        concat_axis=0,
        tiled=True,
    )
    arrived = lax.all_gather(moved_rows, FS, axis=2, tiled=True)
    arranged = arrived.reshape(groups, local_count, capacity, model_width)
    activations = []
    for expert_index in range(local_count):
        expert_rows = arranged[:, expert_index].reshape(groups * capacity, model_width)
        gate_pre = jnp.dot(
            expert_rows, gate_serve[expert_index], preferred_element_type=jnp.float32
        )
        up_pre = jnp.dot(expert_rows, up_serve[expert_index], preferred_element_type=jnp.float32)
        activations.append((jax.nn.silu(gate_pre) * up_pre).astype(jnp.bfloat16))
    stacked = jnp.stack(activations)
    summed = sum_by_chip_2(
        jnp.einsum("jdh,jsh->djs", down_serve, stacked, preferred_element_type=jnp.float32).astype(
            jnp.bfloat16
        ),
        ("fs_0", "fs_1"),
        "fs_2",
        0,
    ).astype(jnp.float32)
    results = summed.astype(jnp.bfloat16).reshape(pieces, local_count, groups, capacity)
    returned = lax.all_to_all(results, "tp", split_axis=2, concat_axis=1, tiled=True)
    flat_out = returned.reshape(pieces, experts * capacity)
    picked = jnp.take(flat_out, slot_ids, axis=1).reshape(pieces, tokens, 2).astype(jnp.float32)
    combined = jnp.sum(picked * weights[None, :, :], axis=2)
    return (gate_serve, up_serve, down_serve, jnp.transpose(combined).astype(jnp.bfloat16))


def solution(mesh):
    split = Mesh(mesh.devices.reshape(4, 4, 2, mesh.shape["tp"]), ("fs_0", "fs_1", "fs_2", "tp"))
    in_specs = (
        P("tp", FS),
        P(FS),
        P(None, FS, "tp"),
        P(None, FS, "tp"),
        P(None, FS, "tp"),
        P("tp", None),
        P("tp", None),
    )
    out_specs = (P("tp", None, FS), P("tp", None, FS), P("tp", None, FS), P("tp", FS))
    return jax.shard_map(
        per_device, mesh=split, in_specs=in_specs, out_specs=out_specs, check_vma=False
    )
```

profile of v0, /device:TPU:1, one launch (start us, length us, event | category | flops | bytes accessed | tf_op | source)
XLA Modules:
  0.0 408.9 jit_solution(17982874354832296313)
XLA Ops:
  8.7 9.6 %all-to-all-start.2 = ((f32[32,1,512]{2,1,0:T(1,128)}), f32[32,1,512]{2,1,0:T(1,128)S(1)}, u32[]{:S(2)}, u32[]{:S(2)}) async-start(f32[32,1,512]{2,1,0:T(1,128)} %broadcast_in_dim.10), calls=%async_computation.2 | async-start | bytes 131072 | tf_op jit(solution)/shard_map/all_to_all | solution.py:30
  27.3 9.6 %all_to_all.49 = bf16[4,512,64]{1,2,0:T(8,128)(2,1)S(1)} all-to-all(bf16[4,512,64]{1,2,0:T(8,128)(2,1)S(1)} %bitcast.115), channel_id=1, replica_groups=mesh['fs_0'=4,'fs_1'=4,'fs_2'=2,'tp'=4] {'tp'}, dimensions={0} | all-to-all | bytes 524288 | tf_op jit(solution)/shard_map/all_to_all | solution.py:114
  38.1 5.1 %multiply_convert_fusion.1 = (bf16[8,64,1792]{2,1,0:T(8,128)(2,1)}, bf16[8,64,1792]{2,1,0:T(8,128)(2,1)S(1)}) fusion(f32[8,64,1792]{2,1,0:T(8,128)} %param.9, f32[64]{0:T(128)S(1)} %copy-done.4, f32[8,64,1792]{2,1,0:T(8,128)} %param.10), kind=kLoop, calls=%fused_computation.8 | loop fusion | flops 3670016 | bytes 11010304 | tf_op jit(solution)/shard_map/convert_element_type | solution.py:82
  43.3 4.0 reshape_reshape.13
  47.3 2.4 convert_element_type.57
  49.7 4.1 reshape_reshape.14
  53.7 4.4 %reshape_reshape.12 = bf16[4,2,64,8,224]{4,3,2,1,0:T(8,128)(2,1)S(1)} reshape(bf16[8,64,1792]{2,1,0:T(8,128)(2,1)} %get-tuple-element.38) | data formatting | bytes 3670016 | tf_op jit(solution)/shard_map/reshape;reshape | solution.py:58
  61.5 4.4 %pad_maximum_fusion = bf16[4,24,2,64,224]{4,3,2,1,0:T(8,128)(2,1)S(1)} fusion(bf16[4,8,2,64,224]{4,3,2,1,0:T(8,128)(2,1)S(1)} %get-tuple-element.40, bf16[4,8,2,64,224]{4,3,2,1,0:T(8,128)(2,1)S(1)} %get-tuple-element.41, bf16[4,8,2,64,224]{4,3,2,1,0:T(8,128)(2,1)S(1)} %bitcast.104), kind=kLoop, calls=%fused_computation.4 | loop fusion | flops 5505024 | bytes 11010048 | tf_op jit(solution)/shard_map/concatenate | solution.py:18
  65.9 72.3 %all_to_all.50 = bf16[4,24,2,64,224]{4,3,2,1,0:T(8,128)(2,1)S(1)} all-to-all(bf16[4,24,2,64,224]{4,3,2,1,0:T(8,128)(2,1)S(1)} %pad_maximum_fusion), channel_id=1, replica_groups=mesh['fs_0'=4,'fs_1'=4,'fs_2'=2,'tp'=4] {'tp'}, dimensions={0} | all-to-all | bytes 11010048 | tf_op jit(solution)/shard_map/all_to_all | solution.py:21
  140.6 82.5 %all_to_all.51 = bf16[32,6,64,224]{3,2,1,0:T(8,128)(2,1)S(1)} all-to-all(bf16[32,6,64,224]{3,2,1,0:T(8,128)(2,1)S(1)} %pad_maximum_fusion.1), channel_id=1, replica_groups=mesh['fs_0'=4,'fs_1'=4,'fs_2'=2,'tp'=4] {'fs_0','fs_1','fs_2'}, dimensions={0} | all-to-all | bytes 11010048 | tf_op jit(solution)/shard_map/all_to_all | solution.py:21
  223.1 3.2 copy.107
  226.4 13.9 %copy.116 = bf16[4,512,2048]{2,1,0:T(8,128)(2,1)} copy(bf16[4,512,2048]{1,0,2:T(4,128)(2,1)} %all-gather.2.cloned.1.call-done) | data formatting | bytes 16777216 | tf_op jit(solution)/shard_map/all_gather | solution.py:121
  240.2 4.1 %fusion.26 = (bf16[4,1,256,2048]{3,2,1,0:T(8,128)(2,1)S(1)}, bf16[4,1,256,2048]{3,2,1,0:T(8,128)(2,1)S(1)}) fusion(bf16[4,2,256,2048]{3,2,1,0:T(8,128)(2,1)} %bitcast.101), kind=kLoop, calls=%fused_computation.61 | loop fusion | bytes 16777216 | tf_op jit(solution)/shard_map/slice | solution.py:125
  250.8 5.8 %convert_bitcast_fusion = bf16[2048,2,1024]{0,2,1:T(8,128)(2,1)} fusion(bf16[1,1024,224]{1,2,0:T(8,128)(2,1)S(1)} %fusion.5, bf16[1,1024,224]{1,2,0:T(8,128)(2,1)S(1)} %fusion.6, bf16[1,6,2048,224]{3,2,1,0:T(8,128)(2,1)S(1)} %bitcast.99), kind=kOutput, calls=%fused_computation.1 | convolution fusion | flops 1883701248 | bytes 11403264 | tf_op jit(solution)/shard_map/jdh,jsh->djs/dot_general | solution.py:133
  256.6 11.8 %copy.117 = bf16[2048,2,1024]{2,0,1:T(8,128)(2,1)} copy(bf16[2048,2,1024]{0,2,1:T(8,128)(2,1)} %convert_bitcast_fusion) | data formatting | bytes 16777216 | tf_op jit(solution)/shard_map/convert_element_type | solution.py:133
  268.4 8.4 %copy.118 = bf16[2,16,64,2,1024]{4,2,3,1,0:T(8,128)(2,1)} copy(bf16[2,16,64,2,1024]{4,2,0,1,3:T(8,128)(2,1)} %bitcast.102) | data formatting | bytes 16777216 | tf_op jit(solution)/shard_map/transpose | solution.py:49
  276.9 15.9 %reduce-scatter.5.cloned.1.call-done = bf16[16,64,2,1024]{3,1,2,0:T(8,128)(2,1)} async-done(((bf16[32,64,2,1024]{3,1,2,0:T(8,128)(2,1)}), bf16[16,64,2,1024]{3,1,2,0:T(8,128)(2,1)}) %reduce-scatter.5.cloned.1.call-update) | async-done | bytes 4194320 | tf_op jit(solution)/shard_map/reduce_scatter | solution.py:50
  293.6 80.5 %reduce-scatter.7.cloned.1.call-done = bf16[1,64,2,1024]{3,1,2,0:T(8,128)(2,1)} async-done(((bf16[16,64,2,1024]{3,1,2,0:T(8,128)(2,1)}), bf16[1,64,2,1024]{3,1,2,0:T(8,128)(2,1)}) %reduce-scatter.7.cloned.1.call-update) | async-done | bytes 262160
  376.0 4.0 all-to-all-start.4
  380.0 5.2 %fusion.27 = (bf16[1,2,2048,224]{3,2,1,0:T(8,128)(2,1)}, bf16[2,2048,224]{2,1,0:T(8,128)(2,1)S(1)}, bf16[2,2048,224]{2,1,0:T(8,128)(2,1)}) fusion(bf16[1,6,2048,224]{3,2,1,0:T(8,128)(2,1)} %bitcast.92), kind=kLoop, calls=%fused_computation.62 | loop fusion | bytes 11010048 | tf_op jit(solution)/shard_map/split | solution.py:20
  385.2 3.9 copy.127
  389.1 3.9 copy.123
  395.5 3.2 gather_fusion
  398.7 2.9 multiply_reduce_fusion
  (67 shorter events, 29.8 us)
Async XLA Ops:
  7.2 30.9 %copy-start.4 = (f32[64]{0:T(128)S(1)}, f32[64]{0:T(128)}, u32[]{:S(2)}) copy-start(f32[64]{0:T(128)} %param.8) | copy-start | bytes 772
  8.7 16.9 %all-to-all-start.2 = ((f32[32,1,512]{2,1,0:T(1,128)}), f32[32,1,512]{2,1,0:T(1,128)S(1)}, u32[]{:S(2)}, u32[]{:S(2)}) async-start(f32[32,1,512]{2,1,0:T(1,128)} %broadcast_in_dim.10), calls=%async_computation.2 | async-start | bytes 131072 | tf_op jit(solution)/shard_map/all_to_all | solution.py:30
  18.3 208.0 %all-gather.2.cloned.1.call-start = ((), (), s32[]{:S(2)}) async-start(), calls=%async_computation.7 | async-start | bytes 8650752 | tf_op jit(solution)/shard_map/all_gather | solution.py:121
  37.9 254.9 %reduce-scatter.5.cloned.1.call-start = ((), (), s32[]{:S(2)}) async-start(), calls=%async_computation.8 | async-start | bytes 12582912 | tf_op jit(solution)/shard_map/reduce_scatter | solution.py:50
  58.1 1.6 copy-start
  58.1 2.2 copy-start.1
  226.4 18.0 %slice-start = ((s8[6291456]{0:T(1024)(128)(4,1)}), s8[2097152]{0:T(1024)(128)(4,1)S(1)}, s32[]{:S(2)}) async-start(s8[6291456]{0:T(1024)(128)(4,1)} %bitcast.93), calls=%async_computation.10 | async-start | bytes 4194304
  240.2 4.7 %slice-start.1 = ((s8[6291456]{0:T(1024)(128)(4,1)}), s8[4194304]{0:T(1024)(128)(4,1)S(1)}, s32[]{:S(2)}) async-start(s8[6291456]{0:T(1024)(128)(4,1)} %bitcast.93), calls=%async_computation.11 | async-start | bytes 8388608
  276.9 16.0 %copy-start.2 = (s32[512,2]{0,1:T(2,128)S(1)}, s32[512,2]{0,1:T(2,128)}, u32[]{:S(2)}) copy-start(s32[512,2]{0,1:T(2,128)} %param.12) | copy-start | bytes 12292
  276.9 16.5 %copy-start.3 = (f32[512,2]{0,1:T(2,128)S(1)}, f32[512,2]{0,1:T(2,128)}, u32[]{:S(2)}) copy-start(f32[512,2]{0,1:T(2,128)} %param.13) | copy-start | bytes 12292
  276.9 97.3 %reduce-scatter.7.cloned.1.call-start = ((), (), s32[]{:S(2)}) async-start(), calls=%async_computation.9 | async-start | bytes 4456448
  376.0 19.2 %all-to-all-start.4 = ((bf16[64,2,4,256]{3,0,1,2:T(8,128)(2,1)}), bf16[64,2,4,256]{3,0,1,2:T(8,128)(2,1)S(1)}, u32[]{:S(2)}, u32[]{:S(2)}) async-start(bf16[64,2,4,256]{3,0,1,2:T(8,128)(2,1)} %copy.119), calls=%async_computation.5 | async-start | bytes 524288 | tf_op jit(solution)/shard_map/all_to_all | solution.py:141
Sparse Core Ops, SparseCore 0:
  38.0 53.6 all-gather.1
  277.0 15.7 reduce-scatter.4
  296.1 77.9 reduce-scatter.6
where the time goes:
time: 412 us; the launch traced here: 409 us
  blocking collectives  164 us (40%)
  waiting for transfers between devices  96.6 us (23%)
  local copies, waits for them, and re-layouts  84.3 us (20%)
  other arithmetic  22.5 us (5%)
  between operations  14.1 us (3%)
  starting transfers between devices  13.9 us (3%)
  matrix products  13.3 us (3%)
    all_to_all x2, blocking collectives, side_by_side(): lax.all_to_all(both, axis, split_axis=split_dim, concat_axis=concat_dim,...  155 us
    unnamed x4, waiting for transfers between devices  80.6 us
    reduce_scatter x1, waiting for transfers between devices, sum_by_chip_2(): tiles = lax.psum_scatter(tiles, core, scatter_dimension=0, tiled=True)  15.9 us
    all_gather x1, local copies, waits for them, and re-layouts, per_device(): arrived = lax.all_gather(moved_rows, FS, axis=2, tiled=True)  13.9 us
    unnamed x19, local copies, waits for them, and re-layouts  13.9 us
    another operation x4, local copies, waits for them, and re-layouts, arrange(): split.reshape(groups, experts // groups, rows, blocks, columns // blocks)  13 us
    convert_element_type x1, local copies, waits for them, and re-layouts, per_device(): jnp.einsum('jdh,jsh->djs', down_serve, stacked, preferred_element_type=jn...  11.8 us
    all_to_all x1, blocking collectives, per_device(): lax.all_to_all(packed.reshape(groups, local_count * capacity, pieces), 't...  9.61 us
  transfers between devices with their start and end apart: 5, of which 3 were waited for; matrix products, arithmetic and copies ran while one was open for 13% of the time, Pallas kernels for 0%

commit v1 on v0

v1 whole, which is shorter than its diff:
```python
import functools

import jax
import jax.numpy as jnp
from jax import lax
from jax.experimental import pallas as pl
from jax.experimental.pallas import tpu as pltpu
from jax.sharding import Mesh
from jax.sharding import PartitionSpec as P

MESH = pl.DeviceIdType.MESH
EPSILON = 1e-06
FS = ("z", "y", "c")
AXES = ("z", "y", "x")
ORDERS = (("x", "y", "z"), ("y", "z", "x"), ("z", "x", "y"))
ROWS = ((0, 96), (96, 80), (176, 80))
HOPS = (1, 3, 2)
PEERS = tuple((dy, dc) for dy in HOPS + (0,) for dc in (0, 1) if (dy, dc) != (0, 0))


def here():
    return {a: lax.axis_index(a) for a in ("z", "y", "c", "x")}


def along(axis, hop):
    return lax.rem(lax.axis_index(axis) + hop, 4)


def greet(both):
    barrier = pltpu.get_barrier_semaphore()
    peers = [{a: along(a, h)} for a in ("x", "z") for h in HOPS]
    if both:
        peers += [{"y": along("y", dy), "c": lax.rem(lax.axis_index("c") + dc, 2)} for dy, dc in PEERS]
    else:
        peers += [{"y": along("y", h)} for h in HOPS] + [{"c": 1 - lax.axis_index("c")}]
    for peer in peers:
        pl.semaphore_signal(barrier, inc=1, device_id=peer, device_id_type=MESH)
    pl.semaphore_wait(barrier, len(peers))


def push(src, dst, send, recv, peer):
    return pltpu.make_async_remote_copy(
        src_ref=src, dst_ref=dst, send_sem=send, recv_sem=recv, device_id=peer, device_id_type=MESH
    )


def pack(read, p):
    first, r = divmod(7 * p, 4)
    lane = lax.broadcasted_iota(jnp.int32, (64, 128), 1)

    def turned(t):
        v = read(t)
        return pltpu.roll(v, 128 - 32 * r, 1) if r else v

    def joined(t, last):
        a = turned(t)
        if r == 0 or last:
            return a
        return jnp.where(lane < 128 - 32 * r, a, turned(t + 1))

    left = joined(first, False)
    right = joined(first + 1, r <= 1)
    tail = right[48:]
    mixed = [
        jnp.where(lane[:16] < 96, right[16 * i : 16 * i + 16], pltpu.roll(tail, 32 * (3 - i), 1))
        for i in range(3)
    ]
    return left, mixed


def spread(masters, gains, hpad, weights, landed, tokens, weight_out,
           raw, sent, over_x, over_z, near, mine, scales,
           in_sem, xs, xr, zs, zr, ys, yr, own_sem, hs, hr, gs, gr, gcs, gcr, gown, wsem, wr):
    at = here()
    x, y, z, c = at["x"], at["y"], at["z"], at["c"]
    other = {"c": 1 - c}
    loads = []
    for k in range(6):
        cp = pltpu.make_async_copy(masters[k // 2].at[:, k % 2], raw.at[k], in_sem.at[k])
        cp.start()
        loads.append(cp)
    greet(True)
    pending = []
    halves = push(hpad.at[1 - c], near, hs, hr, other)
    halves.start()

    copies = {}
    for i, h in enumerate(HOPS):
        peer = along("x", h)
        cp = push(weights.at[peer], weight_out.at[x], wsem.at[i], wr.at[i], {"x": peer})
        cp.start()
        pending.append(cp)
    own_weight = pltpu.make_async_copy(weights.at[x], weight_out.at[x], own_sem.at[6])
    own_weight.start()

    def pack_chunk(k):
        loads[k].wait()

        def one(to, carry):
            gain = gains[k // 2]

            def read(t):
                return raw[k, to, :, 128 * t : 128 * t + 128] * gain

            for p in range(8):
                left, mixed = pack(read, p)
                piece = jnp.concatenate([left] + mixed, axis=0).astype(jnp.bfloat16)
                sent[k, to, p] = piece

            return carry

        lax.fori_loop(0, 4, one, 0)

    def x_sends(k):
        out = []
        for i, h in enumerate(HOPS):
            peer = along("x", h)
            cp = push(sent.at[k, peer], over_x.at[k, x], xs.at[k, i], xr.at[k, i], {"x": peer})
            cp.start()
            out.append(cp)
        copies["x", k] = out
        over_x[k, x] = sent[k, x]

    pack_chunk(0)
    x_sends(0)
    halves.wait()
    mine[...] = hpad[c] + near[...]
    keep = pltpu.make_async_copy(mine, tokens.at[z, y, x, c], gown)
    keep.start()

    def gather_step(l, s):
        order = ORDERS[l]
        r0, nr = ROWS[l]
        index = [slice(None) if a in order[:s] else at[a] for a in AXES] + [c, pl.ds(r0, nr)]
        src = mine.at[pl.ds(r0, nr)] if s == 0 else tokens.at[tuple(index)]
        out = []
        for i, h in enumerate(HOPS):
            cp = push(src, tokens.at[tuple(index)], gs.at[l, s, i], gr.at[l, s, i],
                      {order[s]: along(order[s], h)})
            cp.start()
            out.append(cp)
        copies["g", l, s] = out

    def gathered(l, s):
        for cp in copies["g", l, s]:
            cp.wait_recv()

    for l in range(3):
        gather_step(l, 0)
    for k in range(1, 6):
        pack_chunk(k)
        x_sends(k)
    keep.wait()
    for l in range(3):
        gathered(l, 0)
        gather_step(l, 1)

    def z_step(k):
        for cp in copies["x", k]:
            cp.wait_recv()
        out = []
        for i, h in enumerate(HOPS):
            peer = along("z", h)
            cp = push(over_x.at[k, peer], over_z.at[k, z], zs.at[k, i], zr.at[k, i], {"z": peer})
            cp.start()
            out.append(cp)
        copies["z", k] = out
        over_z[k, z] = over_x[k, z]

    def y_step(k):
        for cp in copies["z", k]:
            cp.wait_recv()
        out = []
        for i, (dy, dc) in enumerate(PEERS):
            py, pc = along("y", dy), lax.rem(c + dc, 2)
            cp = push(over_z.at[k, :, py * 2 + pc], landed.at[k, :, y, c], ys.at[k, i], yr.at[k, i],
                      {"y": py, "c": pc})
            cp.start()
            out.append(cp)
        copies["y", k] = out
        cp = pltpu.make_async_copy(over_z.at[k, :, y * 2 + c], landed.at[k, :, y, c], own_sem.at[k])
        cp.start()
        copies["own", k] = cp

    def core_step(l):
        gathered(l, 2)
        r0, nr = ROWS[l]
        part = tokens.at[:, :, :, c, pl.ds(r0, nr)]
        cp = push(part, part, gcs.at[l], gcr.at[l], other)
        cp.start()
        copies["core", l] = cp

    z_step(0)
    for l in range(3):
        gathered(l, 1)
        gather_step(l, 2)
    for k in range(1, 6):
        z_step(k)
        y_step(k - 1)
        if k == 4:
            for l in range(3):
                core_step(l)
    y_step(5)

    for cp in pending:
        cp.wait()
    own_weight.wait()
    for l in range(3):
        for s in range(3):
            for cp in copies["g", l, s]:
                cp.wait_send()
        copies["core", l].wait()
    for k in range(6):
        for cp in copies["x", k] + copies["z", k]:
            cp.wait_send()
        for cp in copies["y", k]:
            cp.wait()
        copies["own", k].wait()


def spread_call(gate, up, down, gains, hpad, weights):
    def kernel(g, u, d, *rest):
        spread((g, u, d), *rest)

    any_space = pl.BlockSpec(memory_space=pl.ANY)
    vmem = pl.BlockSpec(memory_space=pltpu.VMEM)
    bf16 = jnp.bfloat16
    dma = pltpu.SemaphoreType.DMA
    return pl.pallas_call(
        kernel,
        out_shape=(
            jax.ShapeDtypeStruct((6, 4, 4, 2, 112, 128), bf16),
            jax.ShapeDtypeStruct((4, 4, 4, 2, 256, 128), bf16),
            jax.ShapeDtypeStruct((4, 8, 512), jnp.float32),
        ),
        in_specs=[any_space] * 3 + [vmem] * 2 + [any_space],
        out_specs=(any_space,) * 3,
        scratch_shapes=[
            pltpu.VMEM((6, 4, 64, 1792), jnp.float32),
            pltpu.VMEM((6, 4, 8, 112, 128), bf16),
            pltpu.VMEM((6, 4, 8, 112, 128), bf16),
            pltpu.VMEM((6, 4, 8, 112, 128), bf16),
            pltpu.VMEM((256, 128), bf16),
            pltpu.VMEM((256, 128), bf16),
            pltpu.VMEM((8, 128), jnp.float32),
            dma((6,)), dma((6, 3)), dma((6, 3)), dma((6, 3)), dma((6, 3)), dma((6, 7)), dma((6, 7)), dma((7,)),
            dma, dma, dma((3, 3, 3)), dma((3, 3, 3)), dma((3,)), dma((3,)), dma, dma((3,)), dma((3,)),
        ],
        compiler_params=pltpu.CompilerParams(
            collective_id=0, has_side_effects=True, vmem_limit_bytes=56 << 20
        ),
        name="spread",
    )(gate, up, down, gains, hpad, weights)


def mixture(landed, tokens, weights, gate_out, up_out, down_out, part_out,
            packed, rows, parts, serve, wide, wcol, in_sem, row_sem, w_sem, out_sem, part_sem, wv):
    outs = (gate_out, up_out, down_out)
    loads = []
    for k in range(6):
        cp = pltpu.make_async_copy(landed.at[k], packed.at[k], in_sem.at[k])
        cp.start()
        loads.append(cp)
    wload = pltpu.make_async_copy(weights, wv, w_sem)
    wload.start()
    row_loads = []
    for t in range(8):
        cp = pltpu.make_async_copy(tokens.at[:, pl.ds(256 * t, 256)], rows.at[:, pl.ds(256 * t, 256)], row_sem.at[t])
        cp.start()
        row_loads.append(cp)
    lane = lax.broadcasted_iota(jnp.int32, (16, 128), 1)
    stores = []
    for k in range(6):
        loads[k].wait()
        m, j = k // 2, k % 2

        def one(f, carry):
            serve[m, j, pl.ds(f * 64, 64), 0:128] = packed[k, f, 0:64]
            mixed = packed[k, f, 64:112]
            serve[m, j, pl.ds(f * 64, 48), 128:224] = mixed[:, :96]
            v = mixed.astype(jnp.float32)
            a, b, d = (pltpu.roll(v[16 * i : 16 * i + 16], 32 * (i + 1), 1) for i in range(3))
            tail = jnp.where(lane < 32, a, jnp.where(lane < 64, b, d))
            serve[m, j, pl.ds(f * 64 + 48, 16), 128:224] = tail.astype(jnp.bfloat16)[:, :96]
            return carry

        lax.fori_loop(0, 32, one, 0)
        if j == 1:
            cp = pltpu.make_async_copy(serve.at[m], outs[m], out_sem.at[m])
            cp.start()
            stores.append(cp)
    wload.wait()
    for b in range(4):
        wcol[pl.ds(512 * b, 512), 0:8] = jnp.transpose(wv[b])
    part_stores = []
    for t in range(8):
        row_loads[t].wait()

        total = jnp.zeros((256, 128), jnp.float32)
        for q in range(16):
            block = rows[q, 256 * t : 256 * t + 256]
            wide[:, 128 * q : 128 * q + 128] = block
            v = block.astype(jnp.float32)
            total = total + v * v
        mean = jnp.sum(total, axis=1, keepdims=True) / 2048.0
        inv = lax.rsqrt(mean + EPSILON)
        acts = []
        for e in range(2):
            gate_pre = jnp.dot(wide[...], serve[0, e], preferred_element_type=jnp.float32) * inv
            up_pre = jnp.dot(wide[...], serve[1, e], preferred_element_type=jnp.float32) * inv
            act = gate_pre / (1.0 + jnp.exp(-gate_pre)) * up_pre
            share = wcol[256 * t : 256 * t + 256, e : e + 1]
            acts.append((act * share).astype(jnp.bfloat16))
        dims = (((1,), (1,)), ((), ()))
        for n in range(4):
            cols = slice(512 * n, 512 * n + 512)
            out = lax.dot_general(acts[0], serve[2, 0, cols], dims, preferred_element_type=jnp.float32)
            out = out + lax.dot_general(acts[1], serve[2, 1, cols], dims, preferred_element_type=jnp.float32)
            for q in range(4):
                parts[4 * n + q, 256 * t : 256 * t + 256] = out[:, 128 * q : 128 * q + 128].astype(jnp.bfloat16)
        cp = pltpu.make_async_copy(parts.at[:, pl.ds(256 * t, 256)], part_out.at[:, pl.ds(256 * t, 256)], part_sem.at[t])
        cp.start()
        part_stores.append(cp)
    for cp in stores + part_stores:
        cp.wait()


def mixture_call(landed, tokens, weights):
    any_space = pl.BlockSpec(memory_space=pl.ANY)
    bf16 = jnp.bfloat16
    dma = pltpu.SemaphoreType.DMA
    served = jax.ShapeDtypeStruct((2, 2048, 224), bf16)
    return pl.pallas_call(
        mixture,
        out_shape=(served, served, served, jax.ShapeDtypeStruct((16, 2048, 128), bf16)),
        in_specs=[any_space] * 3,
        out_specs=(any_space,) * 4,
        scratch_shapes=[
            pltpu.VMEM((6, 32, 112, 128), bf16),
            pltpu.VMEM((16, 2048, 128), bf16),
            pltpu.VMEM((16, 2048, 128), bf16),
            pltpu.VMEM((3, 2, 2048, 224), bf16),
            pltpu.VMEM((256, 2048), bf16),
            pltpu.VMEM((2048, 128), jnp.float32),
            dma((6,)), dma((8,)), dma, dma((3,)), dma((8,)),
            pltpu.VMEM((4, 8, 512), jnp.float32),
        ],
        compiler_params=pltpu.CompilerParams(vmem_limit_bytes=60 << 20),
        name="mixture",
    )(landed, tokens, weights)


def collect(parts, out, near, held, one0, one1, one2, two0, two1, two2, three0, three1, three2,
            add0, add1, add2, sum0, sum1, sum2, last,
            load_sem, cs, cr, s_send, s_recv, f_send, f_recv):
    at = here()
    c = at["c"]
    other = {"c": 1 - c}
    greet(False)
    ones, twos, threes = (one0, one1, one2), (two0, two1, two2), (three0, three1, three2)
    adds, sums = (add0, add1, add2), (sum0, sum1, sum2)
    swaps, loads = [], []
    for l in range(3):
        rows = pl.ds(*ROWS[l])
        cp = push(parts.at[:, :, :, 1 - c, rows], near.at[:, :, :, rows], cs.at[l], cr.at[l], other)
        cp.start()
        swaps.append(cp)
        cp = pltpu.make_async_copy(parts.at[:, :, :, c, rows], held.at[:, :, :, rows], load_sem.at[l])
        cp.start()
        loads.append(cp)
    sends = []

    def send(l, s, pick, dst):
        axis = ORDERS[l][s]
        out = []
        for i, h in enumerate(HOPS):
            peer = along(axis, h)
            cp = push(pick(peer), dst.at[i], s_send.at[l, s, i], s_recv.at[l, s, i], {axis: peer})
            cp.start()
            out.append(cp)
        sends.append(out)
        return out

    first, second, third = [], [], []
    for l in range(3):
        r0, nr = ROWS[l]
        swaps[l].wait_recv()
        loads[l].wait()

        def add(i, carry):
            a, b, d = i // 16, lax.rem(i // 4, 4), lax.rem(i, 4)
            v = held[a, b, d, pl.ds(r0, nr)].astype(jnp.float32) + near[a, b, d, pl.ds(r0, nr)].astype(jnp.float32)
            held[a, b, d, pl.ds(r0, nr)] = v.astype(jnp.bfloat16)
            return carry

        lax.fori_loop(0, 64, add, 0)

        def pick(peer, l=l, r0=r0, nr=nr):
            index = [peer if a == ORDERS[l][0] else slice(None) for a in AXES] + [pl.ds(r0, nr)]
            return held.at[tuple(index)]

        first.append(send(l, 0, pick, ones[l]))
    for l in range(3):
        r0, nr = ROWS[l]
        for cp in first[l]:
            cp.wait_recv()
        rest = [a for a in AXES if a != ORDERS[l][0]]

        def add(i, carry):
            a, b = i // 4, lax.rem(i, 4)
            place = {rest[0]: a, rest[1]: b, ORDERS[l][0]: at[ORDERS[l][0]]}
            v = held[place["z"], place["y"], place["x"], pl.ds(r0, nr)].astype(jnp.float32)
            for j in range(3):
                v = v + ones[l][j, a, b].astype(jnp.float32)
            adds[l][a, b] = v.astype(jnp.bfloat16)
            return carry

        lax.fori_loop(0, 16, add, 0)

        def pick(peer, l=l, rest=rest):
            return adds[l].at[peer] if rest[0] == ORDERS[l][1] else adds[l].at[:, peer]

        second.append(send(l, 1, pick, twos[l]))
    for l in range(3):
        for cp in second[l]:
            cp.wait_recv()
        rest = [a for a in AXES if a != ORDERS[l][0]]
        lead = rest[0] == ORDERS[l][1]
        own = at[ORDERS[l][1]]
        for b in range(4):
            v = (adds[l][own, b] if lead else adds[l][b, own]).astype(jnp.float32)
            for j in range(3):
                v = v + twos[l][j, b].astype(jnp.float32)
            sums[l][b] = v.astype(jnp.bfloat16)
        third.append(send(l, 2, lambda peer, l=l: sums[l].at[peer], threes[l]))
    for l in range(3):
        r0, nr = ROWS[l]
        for cp in third[l]:
            cp.wait_recv()
        v = sums[l][at[ORDERS[l][2]]].astype(jnp.float32)
        for j in range(3):
            v = v + threes[l][j].astype(jnp.float32)
        last[pl.ds(r0, nr)] = v.astype(jnp.bfloat16)
    final = push(last, out.at[c], f_send, f_recv, other)
    final.start()
    out[c] = last[...]
    final.wait()
    for cp in swaps:
        cp.wait_send()
    for group in sends:
        for cp in group:
            cp.wait_send()


def collect_call(parts):
    bf16 = jnp.bfloat16
    dma = pltpu.SemaphoreType.DMA
    sizes = [nr for _, nr in ROWS]
    return pl.pallas_call(
        collect,
        out_shape=jax.ShapeDtypeStruct((2, 256, 128), bf16),
        in_specs=[pl.BlockSpec(memory_space=pl.ANY)],
        out_specs=pl.BlockSpec(memory_space=pltpu.VMEM),
        scratch_shapes=[pltpu.VMEM((4, 4, 4, 256, 128), bf16)] * 2
        + [pltpu.VMEM((3, 4, 4, nr, 128), bf16) for nr in sizes]
        + [pltpu.VMEM((3, 4, nr, 128), bf16) for nr in sizes]
        + [pltpu.VMEM((3, nr, 128), bf16) for nr in sizes]
        + [pltpu.VMEM((4, 4, nr, 128), bf16) for nr in sizes]
        + [pltpu.VMEM((4, nr, 128), bf16) for nr in sizes]
        + [
            pltpu.VMEM((256, 128), bf16),
            dma((3,)), dma((3,)), dma((3,)), dma((3, 3, 3)), dma((3, 3, 3)), dma, dma,
        ],
        compiler_params=pltpu.CompilerParams(
            collective_id=1, has_side_effects=True, vmem_limit_bytes=40 << 20
        ),
        name="collect",
    )(parts)


def per_device(hidden, norm_gain, gate_master, up_master, down_master, expert_ids, route_logits):
    c = lax.axis_index("c")
    gains = jnp.stack([norm_gain, norm_gain, jnp.ones_like(norm_gain)])[:, :, None]
    gains = jnp.broadcast_to(gains, (3, 64, 128))
    zero = jnp.zeros_like(hidden)
    lanes = jnp.where(
        c == 0, jnp.concatenate([hidden, zero], axis=1), jnp.concatenate([zero, hidden], axis=1)
    )
    hpad = lanes.reshape(2, 256, 128)
    weights = jax.nn.softmax(route_logits, axis=1)
    chosen = expert_ids[:, :, None] == jnp.arange(8, dtype=jnp.int32)[None, None, :]
    shares = jnp.sum(jnp.where(chosen, weights[:, :, None], 0.0), axis=1)
    shares = jnp.transpose(shares).reshape(4, 2, 512)
    shares = jnp.concatenate([shares, jnp.zeros((4, 6, 512), jnp.float32)], axis=1)
    masters = [m.reshape(4, 2, 64, 1792) for m in (gate_master, up_master, down_master)]
    landed, tokens, shares = spread_call(*masters, gains, hpad, shares)
    gate, up, down, parts = mixture_call(
        landed.reshape(6, 32, 112, 128), tokens.reshape(16, 2048, 128), shares
    )
    out = collect_call(parts.reshape(4, 4, 4, 2, 256, 128)).reshape(512, 128)
    combined = jnp.where(c == 0, out[:, :64], out[:, 64:])
    return gate, up, down, combined


def solution(mesh):
    split = Mesh(mesh.devices.reshape(4, 4, 2, mesh.shape["tp"]), ("z", "y", "c", "x"))
    weight = P(None, FS, "x")
    in_specs = (P("x", FS), P(FS), weight, weight, weight, P("x", None), P("x", None))
    served = P("x", None, FS)
    return jax.shard_map(
        per_device,
        mesh=split,
        in_specs=in_specs,
        out_specs=(served, served, served, P("x", FS)),
        check_vma=False,
    )
```

time: 412 us -> 249 us (0.60)
  Pallas kernels: 0 us -> 227 us
  blocking collectives: 164 us -> 0 us
  waiting for transfers between devices: 96.6 us -> 0 us
  local copies, waits for them, and re-layouts: 84.3 us -> 16 us
  other arithmetic: 22.5 us -> 5.19 us
  starting transfers between devices: 13.9 us -> 0 us
  between operations: 14.1 us -> 0.7 us
  matrix products: 13.3 us -> 0 us
    pallas_call x0 -> x3, Pallas kernels: none -> 227 us  [the longest x1 153 us: spread_call(): pl.pallas_call(kernel, out_shape=(jax.ShapeDtypeStruct((6, 4, 4, 2, 112,...]
    all_to_all x3 -> x0, blocking collectives: 164 us -> none  [the longest x2 155 us: side_by_side(): lax.all_to_all(both, axis, split_axis=split_dim, concat_axis=concat_dim,...]
    unnamed x4 -> x0, waiting for transfers between devices: 80.6 us -> none
    reduce_scatter x1 -> x0, waiting for transfers between devices: 15.9 us -> none  [sum_by_chip_2(): tiles = lax.psum_scatter(tiles, core, scatter_dimension=0, tiled=True)]
    all_gather x1 -> x0, local copies, waits for them, and re-layouts: 13.9 us -> none  [per_device(): arrived = lax.all_gather(moved_rows, FS, axis=2, tiled=True)]
    all_to_all x2 -> x0, starting transfers between devices: 13.6 us -> none  [the longest x1 9.59 us: from_everyone(): lax.all_to_all(jnp.broadcast_to(shard[None], (length, *shard.shape)), axi...]
    dot_general x6 -> x0, matrix products: 13.3 us -> none  [the longest x1 5.81 us: per_device(): jnp.einsum('jdh,jsh->djs', down_serve, stacked, preferred_element_type=jn...]
    another operation x4 -> x1, local copies, waits for them, and re-layouts: 13 us -> 0.07 us  [per_device(): jnp.stack([norm_gain, norm_gain, jnp.ones_like(norm_gain)])[:, :, None]]
  transfers between devices with their start and end apart: 5 -> 0, of which waited for: 3 -> 0; matrix products, arithmetic and copies ran while one was open for 13% -> 0% of each run, Pallas kernels for 0% -> 0%
where the time goes in v1:
time: 249 us
  Pallas kernels  227 us (91%)
  local copies, waits for them, and re-layouts  16 us (6%)
  other arithmetic  5.19 us (2%)
    pallas_call x1, Pallas kernels, spread_call(): pl.pallas_call(kernel, out_shape=(jax.ShapeDtypeStruct((6, 4, 4, 2, 112,...  153 us
    pallas_call x1, Pallas kernels, collect_call(): pl.pallas_call(collect, out_shape=jax.ShapeDtypeStruct((2, 256, 128), bf1...  38.5 us
    pallas_call x1, Pallas kernels, mixture_call(): pl.pallas_call(mixture, out_shape=(served, served, served, jax.ShapeDtype...  35.1 us
    unnamed x9, local copies, waits for them, and re-layouts  13.7 us

profile of v1, /device:TPU:1, one launch (start us, length us, event | category | flops | bytes accessed | tf_op | source)
XLA Modules:
  0.0 248.8 jit_solution(3727089562322577715)
XLA Ops:
  0.6 0.1 pad.5.clone
  0.7 0.8 maximum_maximum_fusion
  1.5 0.7 reduce_max.9
  2.2 0.7 fusion.1
  2.9 0.7 fusion
  3.6 0.7 select_reduce_fusion
  4.3 0.6 concatenate.11.rest_2_
  5.0 0.7 broadcast_in_dim.10.rest_0_
  5.7 0.9 pad_select_fusion
  6.7 0.8 copy.19
  7.4 153.2 %spread.1 = (bf16[6,4,4,2,112,128]{5,4,3,2,1,0:T(8,128)(2,1)}, bf16[4,4,4,2,256,128]{5,4,3,2,1,0:T(8,128)(2,1)}, f32[4,8,512]{2,1,0:T(8,128)}) custom-call(f32[4,2,64,1792]{3,2,1,0:T(8,128)} %bitcast.15, f32[4,2,64,1792]{3,2,1,0:T(8,128)} %bitcast.16, f32[4,2,64,1792]{3,2,1,0:T(8,128)} %bitcast.17, f32[3,64,128]{2,1,0:T(8,128)} %broadcast_in_dim.10.rest_0_, ...), custom_call_target="tpu_custom_call" | custom-call | tf_op jit(solution)/shard_map/spread/pallas_call | solution.py:229
  160.6 35.1 %mixture.1 = (bf16[2,2048,224]{2,1,0:T(8,128)(2,1)}, bf16[2,2048,224]{2,1,0:T(8,128)(2,1)}, bf16[2,2048,224]{2,1,0:T(8,128)(2,1)}, bf16[16,2048,128]{2,1,0:T(8,128)(2,1)}) custom-call(bf16[6,32,112,128]{3,2,1,0:T(8,128)(2,1)} %bitcast.14, bf16[16,2048,128]{2,1,0:T(8,128)(2,1)} %bitcast.13, f32[4,8,512]{2,1,0:T(8,128)} %get-tuple-element.13.weights), custom_call_target="tpu_custom_call" | custom-call | tf_op jit(solution)/shard_map/mixture/pallas_call | solution.py:333
  195.8 3.9 %copy.22 = bf16[2,2048,224]{1,2,0:T(8,128)(2,1)} copy(bf16[2,2048,224]{2,1,0:T(8,128)(2,1)} %get-tuple-element.22) | data formatting | bytes 3670016
  199.7 0.0 copy-start
  199.7 3.4 %copy-done = bf16[16,2048,128]{2,1,0:T(8,128)(2,1)S(1)} copy-done((bf16[16,2048,128]{2,1,0:T(8,128)(2,1)S(1)}, bf16[16,2048,128]{2,1,0:T(8,128)(2,1)}, u32[]{:S(2)}) %copy-start) | copy-done | bytes 8388632
  203.1 38.5 %collect.1 = bf16[2,256,128]{2,1,0:T(8,128)(2,1)S(1)} custom-call(bf16[4,4,4,2,256,128]{5,4,3,2,1,0:T(8,128)(2,1)S(1)} %bitcast.11), custom_call_target="tpu_custom_call" | custom-call | tf_op jit(solution)/shard_map/collect/pallas_call | solution.py:459
  241.6 0.0 copy-start.1
  241.6 0.1 fusion.2
  241.7 0.1 copy.26
  241.8 0.1 copy.25
  241.9 0.6 broadcast_select_fusion
  242.6 3.9 %copy.23 = bf16[2,2048,224]{1,2,0:T(8,128)(2,1)} copy(bf16[2,2048,224]{2,1,0:T(8,128)(2,1)} %get-tuple-element.23) | data formatting | bytes 3670016
  246.5 0.0 copy-done.1
  246.5 2.3 copy.24
  (1 shorter events, 0.0 us)
Async XLA Ops:
  199.7 3.4 %copy-start = (bf16[16,2048,128]{2,1,0:T(8,128)(2,1)S(1)}, bf16[16,2048,128]{2,1,0:T(8,128)(2,1)}, u32[]{:S(2)}) copy-start(bf16[16,2048,128]{2,1,0:T(8,128)(2,1)} %get-tuple-element.17) | copy-start | bytes 25165828
  241.6 4.9 %copy-start.1 = (bf16[2,2048,224]{2,1,0:T(8,128)(2,1)S(1)}, bf16[2,2048,224]{2,1,0:T(8,128)(2,1)}, u32[]{:S(2)}) copy-start(bf16[2,2048,224]{2,1,0:T(8,128)(2,1)} %get-tuple-element.24) | copy-start | bytes 5505028

commit v2 on v0

v2 whole, which is shorter than its diff:
```python
import functools

import jax
import jax.numpy as jnp
from jax import lax
from jax.experimental import pallas as pl
from jax.experimental.pallas import tpu as pltpu
from jax.sharding import Mesh
from jax.sharding import PartitionSpec as P

MESH = pl.DeviceIdType.MESH
EPSILON = 1e-06
FS = ("z", "y", "c")
HOPS = (1, 3, 2)
STEPS = HOPS + (0,)
ROWS = ((0, 96), (96, 80), (176, 80))
HALVES = ((0, 128), (128, 128))
CHUNKS = 12


def along(axis, hop):
    return lax.rem(lax.axis_index(axis) + hop, 4)


def greet():
    barrier = pltpu.get_barrier_semaphore()
    c = lax.axis_index("c")
    peers = [{a: along(a, h)} for a in ("x", "z") for h in HOPS]
    peers += [{"y": along("y", h), "c": lax.rem(c + r, 2)} for r in (0, 1) for h in (STEPS if r else HOPS)]
    for peer in peers:
        pl.semaphore_signal(barrier, inc=1, device_id=peer, device_id_type=MESH)
    pl.semaphore_wait(barrier, len(peers))


def push(src, dst, send, recv, peer):
    return pltpu.make_async_remote_copy(
        src_ref=src, dst_ref=dst, send_sem=send, recv_sem=recv, device_id=peer, device_id_type=MESH
    )


def whole(gate, up, down, gain, hpad, shares,
          gate_out, up_out, down_out, out,
          raw, gains, sent, over_x, over_z, served, tokens, beside, near_shares, share_cols,
          wide, acts, give, near, held, one0, one1, one2, add0, add1, add2,
          two0, two1, two2, sum0, sum1, sum2, three0, three1, three2, last,
          ls, ps, pr, credit, xs, xr, zs, zr, ys, yr, hs, hr, ns, nr, ws, wr,
          g0s, g0r, gs, gr, cs, cr, os, ds, dr, f0s, f0r, fs, fr, ss, sr, ts, tr, es, er):
    masters = (gate, up, down)
    outs = (gate_out, up_out, down_out)
    x, y, z, c = (lax.axis_index(a) for a in ("x", "y", "z", "c"))
    other = {"c": 1 - c}
    sends = []

    def start(cp):
        cp.start()
        sends.append(cp)
        return cp

    mine = pl.ds(pl.multiple_of(c * 64, 64), 64)
    loads, pushes = {}, {}

    def fetch(m):
        for i, h in enumerate(STEPS):
            to = along("x", h)
            cp = pltpu.make_async_copy(masters[m].at[to, c], raw.at[m % 2, to, mine], ls.at[m, i])
            cp.start()
            loads[m, i] = cp

    def swap(m):
        for i, h in enumerate(STEPS):
            to = along("x", h)
            pushes[m, i] = start(
                push(masters[m].at[to, 1 - c], raw.at[m % 2, to, mine], ps.at[m, i], pr.at[m, i], other)
            )

    fetch(0)
    fetch(1)
    gains[mine] = gain[...]
    greet()
    halves = start(push(hpad.at[1 - c], beside, hs, hr, other))
    gain_swap = start(push(gain, gains.at[mine], ns, nr, other))
    swap(0)
    share_swaps = []
    for i, h in enumerate(HOPS):
        peer = along("x", h)
        share_swaps.append(start(push(shares.at[peer], near_shares.at[x], ws.at[i], wr.at[i], {"x": peer})))
    near_shares[x] = shares[x]
    swap(1)

    halves.wait_recv()
    tokens[z, y, x, c] = hpad[c] + beside[...]
    flows = {}

    def gather(l, s, axis, index):
        part = tokens.at[index]
        flows[l, s] = []
        for i, h in enumerate(HOPS):
            cp = push(part, part, gs.at[l, s, i], gr.at[l, s, i], {axis: along(axis, h)})
            flows[l, s].append(start(cp))

    def arrived(group):
        for cp in group:
            cp.wait_recv()

    own = tokens.at[z, y, x, c]
    flows["x"] = [
        start(push(own, own, g0s.at[i], g0r.at[i], {"x": along("x", h)})) for i, h in enumerate(HOPS)
    ]
    gain_swap.wait_recv()

    def pack(m):
        for i in range(4):
            loads[m, i].wait()
            pushes[m, i].wait_recv()

        def one(to, carry):
            for t in range(14):
                v = raw[m % 2, to, :, 128 * t : 128 * t + 128]
                if m < 2:
                    v = v * gains[...]
                v = jnp.transpose(v).astype(jnp.bfloat16)
                at = 128 * t
                while at < 128 * t + 128:
                    u, low = divmod(at, 112)
                    n = min(112 - low, 128 * t + 128 - at)
                    a = at - 128 * t
                    sent[m, to, u // 4, (u // 2) % 2, u % 2, low : low + n] = v[a : a + n]
                    at += n
            return carry

        lax.fori_loop(0, 4, one, 0)

    def split(k):
        return k // 4, (k // 2) % 2, k % 2

    def x_step(k):
        m, hh, rc = split(k)
        cc = lax.rem(c + rc, 2)
        flows["x", k] = [
            start(push(sent.at[m, along("x", h), :, cc, hh], over_x.at[k, x], xs.at[k, i], xr.at[k, i],
                       {"x": along("x", h)}))
            for i, h in enumerate(HOPS)
        ]
        over_x[k, x] = sent[m, x, :, cc, hh]

    def z_step(k):
        arrived(flows["x", k])
        flows["z", k] = [
            start(push(over_x.at[k, along("z", h)], over_z.at[k, z], zs.at[k, i], zr.at[k, i],
                       {"z": along("z", h)}))
            for i, h in enumerate(HOPS)
        ]
        over_z[k, z] = over_x[k, z]

    def lanes(zz):
        return pl.ds(pl.multiple_of((zz * 4 + y) * 128, 128), 128)

    def y_step(k):
        m, hh, rc = split(k)
        arrived(flows["z", k])
        rows = pl.ds(hh * 112, 112)
        flows["y", k] = []
        for i, h in enumerate(STEPS if rc else HOPS):
            py = along("y", h)
            peer = {"y": py, "c": lax.rem(c + rc, 2)}
            for zz in range(4):
                push(over_z.at[k, zz, py], served.at[m, c, rows, lanes(zz)],
                     ys.at[k, i], yr.at[k, i], peer).start()
            cp = push(over_z.at[k, :, 0], over_z.at[k, :, 0], ys.at[k, i], yr.at[k, i], peer)
            flows["y", k].append(cp)
            sends.append(cp)
        if rc == 0:
            for zz in range(4):
                served[m, c, rows, lanes(zz)] = over_z[k, zz, y]

    pack(0)
    for k in range(4):
        x_step(k)
    pl.semaphore_signal(credit, inc=1, device_id=other, device_id_type=MESH)
    fetch(2)
    arrived(flows["x"])
    gather(0, 0, "y", (z, y, slice(None), c, pl.ds(*HALVES[0])))
    gather(1, 0, "z", (z, y, slice(None), c, pl.ds(*HALVES[1])))
    pl.semaphore_wait(credit, 1)
    swap(2)
    pack(1)
    for k in range(4, 8):
        x_step(k)
    arrived(flows[0, 0])
    gather(0, 1, "z", (z, slice(None), slice(None), c, pl.ds(*HALVES[0])))
    arrived(flows[1, 0])
    gather(1, 1, "y", (slice(None), y, slice(None), c, pl.ds(*HALVES[1])))
    z_step(0)
    pack(2)
    for k in range(8, 12):
        x_step(k)
    arrived(share_swaps)
    for b in range(4):
        share_cols[pl.ds(512 * b, 512), 0:8] = jnp.transpose(near_shares[b])

    def core_step(l):
        arrived(flows[l, 1])
        part = tokens.at[:, :, :, c, pl.ds(*HALVES[l])]
        flows["c", l] = [start(push(part, part, cs.at[l], cr.at[l], other))]

    stores = []

    def store(m):
        cp = pltpu.make_async_copy(served.at[m], outs[m], os.at[m])
        cp.start()
        stores.append(cp)

    def act_tile(t, carry):
        xb, ch = t // 2, lax.rem(t, 2)
        total = jnp.zeros((256, 128), jnp.float32)
        for q in range(16):
            block = tokens[q // 4, q % 4, xb, ch]
            wide[:, 128 * q : 128 * q + 128] = block
            v = block.astype(jnp.float32)
            total = total + v * v
        inv = lax.rsqrt(jnp.sum(total, axis=1, keepdims=True) / 2048.0 + EPSILON)
        dims = (((1,), (1,)), ((), ()))
        rows = pl.ds(pl.multiple_of(t * 256, 256), 256)
        for e in range(2):
            gate_pre = lax.dot_general(wide[...], served[0, e], dims, preferred_element_type=jnp.float32) * inv
            up_pre = lax.dot_general(wide[...], served[1, e], dims, preferred_element_type=jnp.float32) * inv
            act = gate_pre / (1.0 + jnp.exp(-gate_pre)) * up_pre
            acts[e, rows] = (act * share_cols[rows, e : e + 1]).astype(jnp.bfloat16)
        return carry

    for k in range(1, 10):
        z_step(k)
        y_step(k - 1)
        if k in (6, 7):
            core_step(k - 6)
    for l in range(2):
        arrived(flows["c", l])
    for k in range(8):
        arrived(flows["y", k])
    store(0)
    store(1)
    lax.fori_loop(0, 3, act_tile, 0)
    z_step(10)
    y_step(9)
    lax.fori_loop(3, 6, act_tile, 0)
    z_step(11)
    y_step(10)
    lax.fori_loop(6, 8, act_tile, 0)
    y_step(11)
    for k in range(8, 12):
        arrived(flows["y", k])
    store(2)

    def down_part(t, n):
        rows = pl.ds(pl.multiple_of(t * 256, 256), 256)
        cols = slice(512 * n, 512 * n + 512)
        v = jnp.dot(acts[0, rows], served[2, 0, :, cols], preferred_element_type=jnp.float32)
        return v + jnp.dot(acts[1, rows], served[2, 1, :, cols], preferred_element_type=jnp.float32)

    given = []
    for i, h in enumerate(STEPS):
        t = along("x", h) * 2 + 1 - c
        for n in range(4):
            v = down_part(t, n)
            for b in range(4):
                give[i, n, b] = v[:, 128 * b : 128 * b + 128].astype(jnp.bfloat16)
        given.append(start(push(give.at[i], near.at[i], ds.at[i], dr.at[i], other)))
    r0, r1, r2 = (pl.ds(*r) for r in ROWS)
    first = ([], [], [])
    every = slice(None)
    for i, h in enumerate(STEPS):
        t = along("x", h) * 2 + c
        arrived([given[i]])
        for n in range(4):
            v = down_part(t, n)
            for b in range(4):
                total = v[:, 128 * b : 128 * b + 128] + near[i, n, b].astype(jnp.float32)
                held[n, b, i] = total.astype(jnp.bfloat16)
        if i < 3:
            first[0].append(
                start(push(held.at[every, every, i, r0], one0.at[i], f0s.at[i], f0r.at[i], {"x": along("x", h)}))
            )
        for j, g in enumerate(HOPS):
            py, pz = along("y", g), along("z", g)
            first[1].append(
                start(push(held.at[every, py, i, r1], one1.at[j, :, i], fs.at[0, i, j], fr.at[0, i, j], {"y": py}))
            )
            first[2].append(
                start(push(held.at[pz, every, i, r2], one2.at[j, :, i], fs.at[1, i, j], fr.at[1, i, j], {"z": pz}))
            )

    def summed(base, terms):
        v = base.astype(jnp.float32)
        for term in terms:
            v = v + term.astype(jnp.float32)
        return v

    def add_first(l, one, add, base):
        arrived(first[l])

        def body(n, carry):
            a, b = n // 4, lax.rem(n, 4)
            add[a, b] = summed(base(a, b), [one[j, a, b] for j in range(3)]).astype(jnp.bfloat16)
            return carry

        lax.fori_loop(0, 16, body, 0)

    second, third = [], []
    add_first(0, one0, add0, lambda a, b: held[a, b, 3, r0])
    second.append([
        start(push(add0.at[:, along("y", h)], two0.at[j], ss.at[0, j], sr.at[0, j], {"y": along("y", h)}))
        for j, h in enumerate(HOPS)
    ])
    add_first(1, one1, add1, lambda a, b: held[a, y, b, r1])
    second.append([
        start(push(add1.at[along("z", h)], two1.at[j], ss.at[1, j], sr.at[1, j], {"z": along("z", h)}))
        for j, h in enumerate(HOPS)
    ])
    add_first(2, one2, add2, lambda a, b: held[z, a, b, r2])
    second.append([
        start(push(add2.at[:, j], two2.at[j], ss.at[2, j], sr.at[2, j], {"x": along("x", h)}))
        for j, h in enumerate(HOPS)
    ])

    def add_second(l, two, into, base):
        arrived(second[l])
        for a in range(4):
            into[a] = summed(base(a), [two[j, a] for j in range(3)]).astype(jnp.bfloat16)

    add_second(0, two0, sum0, lambda a: add0[a, y])
    third.append([
        start(push(sum0.at[along("z", h)], three0.at[j], ts.at[0, j], tr.at[0, j], {"z": along("z", h)}))
        for j, h in enumerate(HOPS)
    ])
    add_second(1, two1, sum1, lambda a: add1[z, a])
    third.append([
        start(push(sum1.at[j], three1.at[j], ts.at[1, j], tr.at[1, j], {"x": along("x", h)}))
        for j, h in enumerate(HOPS)
    ])
    add_second(2, two2, sum2, lambda a: add2[a, 3])
    third.append([
        start(push(sum2.at[along("y", h)], three2.at[j], ts.at[2, j], tr.at[2, j], {"y": along("y", h)}))
        for j, h in enumerate(HOPS)
    ])
    for l, (three, base) in enumerate(((three0, sum0[z]), (three1, sum1[3]), (three2, sum2[y]))):
        arrived(third[l])
        last[pl.ds(*ROWS[l])] = summed(base, [three[j] for j in range(3)]).astype(jnp.bfloat16)
    final = start(push(last, out.at[c], es, er, other))
    out[c] = last[...]
    final.wait_recv()
    for cp in sends:
        cp.wait_send()
    for cp in stores:
        cp.wait()


def whole_call(gate, up, down, gain, hpad, shares):
    any_space = pl.BlockSpec(memory_space=pl.ANY)
    vmem = pl.BlockSpec(memory_space=pltpu.VMEM)
    bf16, f32 = jnp.bfloat16, jnp.float32
    dma = pltpu.SemaphoreType.DMA
    sizes = [n for _, n in ROWS]
    served = jax.ShapeDtypeStruct((2, 224, 2048), bf16)

    def buffers(*shapes):
        return [pltpu.VMEM(s, bf16) for s in shapes]

    return pl.pallas_call(
        whole,
        out_shape=(served, served, served, jax.ShapeDtypeStruct((2, 256, 128), bf16)),
        in_specs=[any_space] * 3 + [vmem] * 3,
        out_specs=(any_space,) * 3 + (vmem,),
        scratch_shapes=[pltpu.VMEM((2, 4, 128, 1792), f32), pltpu.VMEM((128, 128), f32)]
        + buffers((3, 4, 4, 2, 2, 112, 128), (CHUNKS, 4, 4, 112, 128), (CHUNKS, 4, 4, 112, 128),
                  (3, 2, 224, 2048), (4, 4, 4, 2, 256, 128), (256, 128))
        + [pltpu.VMEM((4, 8, 512), f32), pltpu.VMEM((2048, 128), f32)]
        + buffers((256, 2048), (2, 2048, 224), (4, 4, 4, 256, 128), (4, 4, 4, 256, 128), (4, 4, 4, 256, 128))
        + buffers(*[(3, 4, 4, n, 128) for n in sizes])
        + buffers(*[(4, 4, n, 128) for n in sizes])
        + buffers(*[(3, 4, n, 128) for n in sizes])
        + buffers(*[(4, n, 128) for n in sizes])
        + buffers(*[(3, n, 128) for n in sizes])
        + buffers((256, 128))
        + [dma((3, 4)), dma((3, 4)), dma((3, 4)), pltpu.SemaphoreType.REGULAR]
        + [dma((CHUNKS, 3))] * 4
        + [dma((CHUNKS, 4))] * 2
        + [dma] * 4
        + [dma((3,))] * 2
        + [dma((3,))] * 2
        + [dma((2, 2, 3))] * 2
        + [dma((2,))] * 2
        + [dma((3,))]
        + [dma((4,))] * 2
        + [dma((3,))] * 2
        + [dma((2, 4, 3))] * 2
        + [dma((3, 3))] * 4
        + [dma] * 2,
        compiler_params=pltpu.CompilerParams(
            collective_id=0, has_side_effects=True, vmem_limit_bytes=67043328
        ),
        name="whole",
    )(gate, up, down, gain, hpad, shares)


def per_device(hidden, norm_gain, gate_master, up_master, down_master, expert_ids, route_logits):
    c = lax.axis_index("c")
    gain = jnp.broadcast_to(norm_gain[:, None], (64, 128))
    zero = jnp.zeros_like(hidden)
    lanes = jnp.where(
        c == 0, jnp.concatenate([hidden, zero], axis=1), jnp.concatenate([zero, hidden], axis=1)
    )
    hpad = lanes.reshape(2, 256, 128)
    weights = jax.nn.softmax(route_logits, axis=1)
    chosen = expert_ids[:, :, None] == jnp.arange(8, dtype=jnp.int32)[None, None, :]
    shares = jnp.sum(jnp.where(chosen, weights[:, :, None], 0.0), axis=1)
    shares = jnp.transpose(shares).reshape(4, 2, 512)
    shares = jnp.concatenate([shares, jnp.zeros((4, 6, 512), jnp.float32)], axis=1)
    masters = [m.reshape(4, 2, 64, 1792) for m in (gate_master, up_master, down_master)]
    gate, up, down, out = whole_call(*masters, gain, hpad, shares)
    out = out.reshape(512, 128)
    combined = jnp.where(c == 0, out[:, :64], out[:, 64:])
    return jnp.swapaxes(gate, 1, 2), jnp.swapaxes(up, 1, 2), jnp.swapaxes(down, 1, 2), combined


def solution(mesh):
    split = Mesh(mesh.devices.reshape(4, 4, 2, mesh.shape["tp"]), ("z", "y", "c", "x"))
    weight = P(None, FS, "x")
    in_specs = (P("x", FS), P(FS), weight, weight, weight, P("x", None), P("x", None))
    served = P("x", None, FS)
    return jax.shard_map(
        per_device,
        mesh=split,
        in_specs=in_specs,
        out_specs=(served, served, served, P("x", FS)),
        check_vma=False,
    )
```

time: 412 us -> 176 us (0.43)
  blocking collectives: 164 us -> 0 us
  Pallas kernels: 0 us -> 160 us
  waiting for transfers between devices: 96.6 us -> 0 us
  local copies, waits for them, and re-layouts: 84.3 us -> 10.5 us
  other arithmetic: 22.5 us -> 4.39 us
  starting transfers between devices: 13.9 us -> 0 us
  between operations: 14.1 us -> 0.67 us
  matrix products: 13.3 us -> 0 us
    all_to_all x3 -> x0, blocking collectives: 164 us -> none  [the longest x2 155 us: side_by_side(): lax.all_to_all(both, axis, split_axis=split_dim, concat_axis=concat_dim,...]
    pallas_call x0 -> x1, Pallas kernels: none -> 160 us  [whole_call(): pl.pallas_call(whole, out_shape=(served, served, served, jax.ShapeDtypeSt...]
    unnamed x4 -> x0, waiting for transfers between devices: 80.6 us -> none
    reduce_scatter x1 -> x0, waiting for transfers between devices: 15.9 us -> none  [sum_by_chip_2(): tiles = lax.psum_scatter(tiles, core, scatter_dimension=0, tiled=True)]
    all_gather x1 -> x0, local copies, waits for them, and re-layouts: 13.9 us -> none  [per_device(): arrived = lax.all_gather(moved_rows, FS, axis=2, tiled=True)]
    all_to_all x2 -> x0, starting transfers between devices: 13.6 us -> none  [the longest x1 9.59 us: from_everyone(): lax.all_to_all(jnp.broadcast_to(shard[None], (length, *shard.shape)), axi...]
    dot_general x6 -> x0, matrix products: 13.3 us -> none  [the longest x1 5.81 us: per_device(): jnp.einsum('jdh,jsh->djs', down_serve, stacked, preferred_element_type=jn...]
    another operation x4 -> x0, local copies, waits for them, and re-layouts: 13 us -> none  [arrange(): split.reshape(groups, experts // groups, rows, blocks, columns // blocks)]
  transfers between devices with their start and end apart: 5 -> 0, of which waited for: 3 -> 0; matrix products, arithmetic and copies ran while one was open for 13% -> 0% of each run, Pallas kernels for 0% -> 0%
where the time goes in v2:
time: 176 us
  Pallas kernels  160 us (91%)
  local copies, waits for them, and re-layouts  10.5 us (6%)
  other arithmetic  4.39 us (2%)
    pallas_call x1, Pallas kernels, whole_call(): pl.pallas_call(whole, out_shape=(served, served, served, jax.ShapeDtypeSt...  160 us
    unnamed x9, local copies, waits for them, and re-layouts  6.66 us

profile of v2, /device:TPU:1, one launch (start us, length us, event | category | flops | bytes accessed | tf_op | source)
XLA Modules:
  0.0 175.8 jit_solution(6266135327550305207)
XLA Ops:
  0.6 0.7 reduce_max.9
  1.3 0.7 fusion.1
  2.0 0.7 fusion
  2.8 0.7 select_reduce_fusion
  3.5 0.6 concatenate.11.shares
  4.1 0.9 pad_select_fusion
  5.0 0.8 copy.16
  5.8 1.3 broadcast_in_dim.10.gain
  7.2 160.2 %whole.1 = (bf16[2,224,2048]{2,1,0:T(8,128)(2,1)}, bf16[2,224,2048]{2,1,0:T(8,128)(2,1)}, bf16[2,224,2048]{2,1,0:T(8,128)(2,1)}, bf16[2,256,128]{2,1,0:T(8,128)(2,1)}) custom-call(f32[4,2,64,1792]{3,2,1,0:T(8,128)} %bitcast.9, f32[4,2,64,1792]{3,2,1,0:T(8,128)} %bitcast.10, f32[4,2,64,1792]{3,2,1,0:T(8,128)} %bitcast.11, f32[64,128]{1,0:T(8,128)} %broadcast_in_dim.10.gain, ...), custom_call_target="tpu_custom_call" | custom-call | tf_op jit(solution)/shard_map/whole/pallas_call | solution.py:368
  167.4 1.1 fusion.2
  168.5 0.1 copy.19
  168.6 0.1 copy.20
  168.7 0.6 broadcast_select_fusion
  169.3 0.0 copy-start.1
  169.3 3.1 %copy.24 = bf16[2,2048,224]{1,2,0:T(8,128)(2,1)} copy(bf16[2,2048,224]{1,2,0:T(8,128)(2,1)} %bitcast.14) | data formatting | bytes 3670016
  172.4 0.0 copy-done.1
  172.4 0.0 copy-start
  172.4 1.2 copy.25
  173.6 0.9 copy-done
  174.5 1.2 copy.26
  (1 shorter events, 0.0 us)
Async XLA Ops:
  169.3 3.1 %copy-start.1 = (bf16[2,224,2048]{2,1,0:T(8,128)(2,1)S(1)}, bf16[2,224,2048]{2,1,0:T(8,128)(2,1)}, u32[]{:S(2)}) copy-start(bf16[2,224,2048]{2,1,0:T(8,128)(2,1)} %get-tuple-element.9) | copy-start | bytes 5505028
  172.4 2.2 %copy-start = (bf16[2,224,2048]{2,1,0:T(8,128)(2,1)S(1)}, bf16[2,224,2048]{2,1,0:T(8,128)(2,1)}, u32[]{:S(2)}) copy-start(bf16[2,224,2048]{2,1,0:T(8,128)(2,1)} %get-tuple-element.10) | copy-start | bytes 5505028

commit v3 on v2

--- a/solution.py
+++ b/solution.py
@@ -38,13 +38,13 @@
     )
 
 
-def whole(gate, up, down, gain, hpad, shares,
+def whole(gate, up, down, gain, hidden, ids, logits,
           gate_out, up_out, down_out, out,
-          raw, gains, sent, over_x, over_z, served, tokens, beside, near_shares, share_cols,
+          raw, gains, sent, over_x, over_z, served, tokens, chip, shares, near_shares, share_cols,
           wide, acts, give, near, held, one0, one1, one2, add0, add1, add2,
-          two0, two1, two2, sum0, sum1, sum2, three0, three1, three2, last,
+          two0, two1, two2, sum0, sum1, sum2, three0, three1, three2, last, turned,
           ls, ps, pr, credit, xs, xr, zs, zr, ys, yr, hs, hr, ns, nr, ws, wr,
-          g0s, g0r, gs, gr, cs, cr, os, ds, dr, f0s, f0r, fs, fr, ss, sr, ts, tr, es, er):
+          g0s, g0r, gs, gr, hops, hopr, cs, cr, os, ds, dr, f0s, f0r, fs, fr, ss, sr, ts, tr, es, er):
     masters = (gate, up, down)
     outs = (gate_out, up_out, down_out)
     x, y, z, c = (lax.axis_index(a) for a in ("x", "y", "z", "c"))
@@ -75,38 +75,88 @@
 
     fetch(0)
     fetch(1)
-    gains[mine] = gain[...]
+    half = pl.ds(pl.multiple_of(c * 256, 256), 256)
+    far_half = pl.ds(pl.multiple_of((1 - c) * 256, 256), 256)
+    chip[mine] = hidden[:, half]
+    lane = lax.broadcasted_iota(jnp.int32, (8, 128), 1)
+    doubled = jnp.broadcast_to(gain[...], (8, 128))
     greet()
-    halves = start(push(hpad.at[1 - c], beside, hs, hr, other))
-    gain_swap = start(push(gain, gains.at[mine], ns, nr, other))
+    halves = start(push(hidden.at[:, far_half], chip.at[mine], hs, hr, other))
+    gain_swap = start(push(gain, gains, ns, nr, other))
     swap(0)
+
+    l0, l1 = logits[0:1], logits[1:2]
+    top = jnp.maximum(l0, l1)
+    e0, e1 = jnp.exp(l0 - top), jnp.exp(l1 - top)
+    w0, w1 = e0 / (e0 + e1), e1 / (e0 + e1)
+    for to in range(4):
+        expert = lax.broadcasted_iota(jnp.int32, (8, 512), 0) + 2 * to
+        shares[to] = jnp.where(ids[0:1] == expert, w0, 0.0) + jnp.where(ids[1:2] == expert, w1, 0.0)
+    near_shares[x] = shares[x]
+    swap(1)
+
+    halves.wait_recv()
+    tokens[z, y, x, c] = jnp.transpose(chip[...].astype(jnp.float32)).astype(jnp.bfloat16)
+    flows = {}
+
+    def arrived(group):
+        for cp in group:
+            cp.wait_recv()
+
+    def spot(axis, at, rows):
+        return (at if axis == "z" else slice(None), at if axis == "y" else slice(None), slice(None), c, rows)
+
+    own = tokens.at[z, y, x, c]
+    flows["x"] = [
+        start(push(own, own, g0s.at[i], g0r.at[i], {"x": along("x", h)})) for i, h in enumerate(HOPS)
+    ]
     share_swaps = []
     for i, h in enumerate(HOPS):
         peer = along("x", h)
         share_swaps.append(start(push(shares.at[peer], near_shares.at[x], ws.at[i], wr.at[i], {"x": peer})))
-    near_shares[x] = shares[x]
-    swap(1)
-
-    halves.wait_recv()
-    tokens[z, y, x, c] = hpad[c] + beside[...]
-    flows = {}
-
-    def gather(l, s, axis, index):
-        part = tokens.at[index]
-        flows[l, s] = []
-        for i, h in enumerate(HOPS):
-            cp = push(part, part, gs.at[l, s, i], gr.at[l, s, i], {axis: along(axis, h)})
-            flows[l, s].append(start(cp))
-
-    def arrived(group):
-        for cp in group:
-            cp.wait_recv()
-
-    own = tokens.at[z, y, x, c]
-    flows["x"] = [
-        start(push(own, own, g0s.at[i], g0r.at[i], {"x": along("x", h)})) for i, h in enumerate(HOPS)
-    ]
     gain_swap.wait_recv()
+    gains[...] = jnp.where((lane < 64) == (c == 0), doubled, gains[...])
+    arrived(flows["x"])
+    for l, axis in enumerate(("y", "z")):
+        part = tokens.at[z, y, slice(None), c, pl.ds(*HALVES[l])]
+        flows["g", l] = [
+            start(push(part, part, gs.at[l, i], gr.at[l, i], {axis: along(axis, h)}))
+            for i, h in enumerate(HOPS)
+        ]
+
+    def spread_out(l):
+        axis = ("z", "y")[l]
+        arrived(flows["g", l])
+        part = tokens.at[spot(axis, lax.axis_index(axis), pl.ds(*HALVES[l]))]
+        flows["n", l] = [
+            start(push(part, part, hops.at[l, i], hopr.at[l, i], {axis: along(axis, h)}))
+            for i, h in enumerate((1, 3))
+        ]
+
+    def pass_on(l):
+        axis = ("z", "y")[l]
+        first, count = HALVES[l]
+        flows["p", l] = []
+        for i, h in enumerate((1, 3)):
+            flows["n", l][i].wait_recv()
+            rows = pl.ds(first + i * (count // 2), count // 2)
+            part = tokens.at[spot(axis, along(axis, 4 - h), rows)]
+            cp = push(part, part, hops.at[l, 2 + i], hopr.at[l, 2 + i], {axis: along(axis, h)})
+            flows["p", l].append(start(cp))
+
+    def pack_one(m, to):
+        for t in range(14):
+            v = jnp.transpose(raw[m % 2, to, :, 128 * t : 128 * t + 128])
+            if m < 2:
+                v = v * gains[0:1]
+            v = v.astype(jnp.bfloat16)
+            at = 128 * t
+            while at < 128 * t + 128:
+                u, low = divmod(at, 112)
+                n = min(112 - low, 128 * t + 128 - at)
+                a = at - 128 * t
+                sent[m, to, u // 4, (u // 2) % 2, u % 2, low : low + n] = v[a : a + n]
+                at += n
 
     def pack(m):
         for i in range(4):
@@ -114,18 +164,7 @@
             pushes[m, i].wait_recv()
 
         def one(to, carry):
-            for t in range(14):
-                v = raw[m % 2, to, :, 128 * t : 128 * t + 128]
-                if m < 2:
-                    v = v * gains[...]
-                v = jnp.transpose(v).astype(jnp.bfloat16)
-                at = 128 * t
-                while at < 128 * t + 128:
-                    u, low = divmod(at, 112)
-                    n = min(112 - low, 128 * t + 128 - at)
-                    a = at - 128 * t
-                    sent[m, to, u // 4, (u // 2) % 2, u % 2, low : low + n] = v[a : a + n]
-                    at += n
+            pack_one(m, to)
             return carry
 
         lax.fori_loop(0, 4, one, 0)
@@ -133,15 +172,23 @@
     def split(k):
         return k // 4, (k // 2) % 2, k % 2
 
-    def x_step(k):
+    def x_send(k, i):
         m, hh, rc = split(k)
-        cc = lax.rem(c + rc, 2)
-        flows["x", k] = [
-            start(push(sent.at[m, along("x", h), :, cc, hh], over_x.at[k, x], xs.at[k, i], xr.at[k, i],
-                       {"x": along("x", h)}))
-            for i, h in enumerate(HOPS)
-        ]
-        over_x[k, x] = sent[m, x, :, cc, hh]
+        peer = along("x", HOPS[i])
+        src = sent.at[m, peer, :, lax.rem(c + rc, 2), hh]
+        flows["x", k].append(start(push(src, over_x.at[k, x], xs.at[k, i], xr.at[k, i], {"x": peer})))
+
+    def x_keep(k):
+        m, hh, rc = split(k)
+        over_x[k, x] = sent[m, x, :, lax.rem(c + rc, 2), hh]
+
+    def x_steps(m):
+        for k in range(4 * m, 4 * m + 4):
+            flows["x", k] = []
+            for i in range(3):
+                x_send(k, i)
+        for k in range(4 * m, 4 * m + 4):
+            x_keep(k)
 
     def z_step(k):
         arrived(flows["x", k])
@@ -173,33 +220,36 @@
             for zz in range(4):
                 served[m, c, rows, lanes(zz)] = over_z[k, zz, y]
 
-    pack(0)
     for k in range(4):
-        x_step(k)
+        flows["x", k] = []
+    for i, h in enumerate(STEPS):
+        loads[0, i].wait()
+        pushes[0, i].wait_recv()
+        pack_one(0, along("x", h))
+        if i < 3:
+            x_send(0, i)
+    for k in range(1, 4):
+        for i in range(3):
+            x_send(k, i)
     pl.semaphore_signal(credit, inc=1, device_id=other, device_id_type=MESH)
     fetch(2)
-    arrived(flows["x"])
-    gather(0, 0, "y", (z, y, slice(None), c, pl.ds(*HALVES[0])))
-    gather(1, 0, "z", (z, y, slice(None), c, pl.ds(*HALVES[1])))
+    for k in range(4):
+        x_keep(k)
+    spread_out(0)
+    spread_out(1)
     pl.semaphore_wait(credit, 1)
     swap(2)
     pack(1)
-    for k in range(4, 8):
-        x_step(k)
-    arrived(flows[0, 0])
-    gather(0, 1, "z", (z, slice(None), slice(None), c, pl.ds(*HALVES[0])))
-    arrived(flows[1, 0])
-    gather(1, 1, "y", (slice(None), y, slice(None), c, pl.ds(*HALVES[1])))
+    x_steps(1)
     z_step(0)
     pack(2)
-    for k in range(8, 12):
-        x_step(k)
+    x_steps(2)
     arrived(share_swaps)
     for b in range(4):
         share_cols[pl.ds(512 * b, 512), 0:8] = jnp.transpose(near_shares[b])
 
     def core_step(l):
-        arrived(flows[l, 1])
+        arrived(flows["p", l])
         part = tokens.at[:, :, :, c, pl.ds(*HALVES[l])]
         flows["c", l] = [start(push(part, part, cs.at[l], cr.at[l], other))]
 
@@ -231,6 +281,9 @@
     for k in range(1, 10):
         z_step(k)
         y_step(k - 1)
+        if k == 2:
+            pass_on(0)
+            pass_on(1)
         if k in (6, 7):
             core_step(k - 6)
     for l in range(2):
@@ -345,8 +398,10 @@
     for l, (three, base) in enumerate(((three0, sum0[z]), (three1, sum1[3]), (three2, sum2[y]))):
         arrived(third[l])
         last[pl.ds(*ROWS[l])] = summed(base, [three[j] for j in range(3)]).astype(jnp.bfloat16)
-    final = start(push(last, out.at[c], es, er, other))
-    out[c] = last[...]
+    turned[...] = jnp.transpose(last[...].astype(jnp.float32)).astype(jnp.bfloat16)
+    rest = turned.at[pl.ds(pl.multiple_of((1 - c) * 64, 64), 64)]
+    final = start(push(rest, out.at[:, half], es, er, other))
+    out[:, half] = turned[mine]
     final.wait_recv()
     for cp in sends:
         cp.wait_send()
@@ -354,7 +409,7 @@
         cp.wait()
 
 
-def whole_call(gate, up, down, gain, hpad, shares):
+def whole_call(gate, up, down, gain, hidden, ids, logits):
     any_space = pl.BlockSpec(memory_space=pl.ANY)
     vmem = pl.BlockSpec(memory_space=pltpu.VMEM)
     bf16, f32 = jnp.bfloat16, jnp.float32
@@ -367,27 +422,29 @@
 
     return pl.pallas_call(
         whole,
-        out_shape=(served, served, served, jax.ShapeDtypeStruct((2, 256, 128), bf16)),
-        in_specs=[any_space] * 3 + [vmem] * 3,
+        out_shape=(served, served, served, jax.ShapeDtypeStruct((64, 512), bf16)),
+        in_specs=[any_space] * 3 + [vmem] * 4,
         out_specs=(any_space,) * 3 + (vmem,),
-        scratch_shapes=[pltpu.VMEM((2, 4, 128, 1792), f32), pltpu.VMEM((128, 128), f32)]
+        scratch_shapes=[pltpu.VMEM((2, 4, 128, 1792), f32), pltpu.VMEM((8, 128), f32)]
         + buffers((3, 4, 4, 2, 2, 112, 128), (CHUNKS, 4, 4, 112, 128), (CHUNKS, 4, 4, 112, 128),
-                  (3, 2, 224, 2048), (4, 4, 4, 2, 256, 128), (256, 128))
-        + [pltpu.VMEM((4, 8, 512), f32), pltpu.VMEM((2048, 128), f32)]
+                  (3, 2, 224, 2048), (4, 4, 4, 2, 256, 128), (128, 256))
+        + [pltpu.VMEM((4, 8, 512), f32)] * 2
+        + [pltpu.VMEM((2048, 128), f32)]
         + buffers((256, 2048), (2, 2048, 224), (4, 4, 4, 256, 128), (4, 4, 4, 256, 128), (4, 4, 4, 256, 128))
         + buffers(*[(3, 4, 4, n, 128) for n in sizes])
         + buffers(*[(4, 4, n, 128) for n in sizes])
         + buffers(*[(3, 4, n, 128) for n in sizes])
         + buffers(*[(4, n, 128) for n in sizes])
         + buffers(*[(3, n, 128) for n in sizes])
-        + buffers((256, 128))
+        + buffers((256, 128), (128, 256))
         + [dma((3, 4)), dma((3, 4)), dma((3, 4)), pltpu.SemaphoreType.REGULAR]
         + [dma((CHUNKS, 3))] * 4
         + [dma((CHUNKS, 4))] * 2
         + [dma] * 4
         + [dma((3,))] * 2
         + [dma((3,))] * 2
-        + [dma((2, 2, 3))] * 2
+        + [dma((2, 3))] * 2
+        + [dma((2, 4))] * 2
         + [dma((2,))] * 2
         + [dma((3,))]
         + [dma((4,))] * 2
@@ -399,27 +456,16 @@
             collective_id=0, has_side_effects=True, vmem_limit_bytes=67043328
         ),
         name="whole",
-    )(gate, up, down, gain, hpad, shares)
+    )(gate, up, down, gain, hidden, ids, logits)
 
 
 def per_device(hidden, norm_gain, gate_master, up_master, down_master, expert_ids, route_logits):
-    c = lax.axis_index("c")
-    gain = jnp.broadcast_to(norm_gain[:, None], (64, 128))
-    zero = jnp.zeros_like(hidden)
-    lanes = jnp.where(
-        c == 0, jnp.concatenate([hidden, zero], axis=1), jnp.concatenate([zero, hidden], axis=1)
+    gain = jnp.broadcast_to(jnp.concatenate([norm_gain, norm_gain])[None, :], (8, 128))
+    masters = [m.reshape(4, 2, 64, 1792) for m in (gate_master, up_master, down_master)]
+    gate, up, down, out = whole_call(
+        *masters, gain, jnp.transpose(hidden), jnp.transpose(expert_ids), jnp.transpose(route_logits)
     )
-    hpad = lanes.reshape(2, 256, 128)
-    weights = jax.nn.softmax(route_logits, axis=1)
-    chosen = expert_ids[:, :, None] == jnp.arange(8, dtype=jnp.int32)[None, None, :]
-    shares = jnp.sum(jnp.where(chosen, weights[:, :, None], 0.0), axis=1)
-    shares = jnp.transpose(shares).reshape(4, 2, 512)
-    shares = jnp.concatenate([shares, jnp.zeros((4, 6, 512), jnp.float32)], axis=1)
-    masters = [m.reshape(4, 2, 64, 1792) for m in (gate_master, up_master, down_master)]
-    gate, up, down, out = whole_call(*masters, gain, hpad, shares)
-    out = out.reshape(512, 128)
-    combined = jnp.where(c == 0, out[:, :64], out[:, 64:])
-    return jnp.swapaxes(gate, 1, 2), jnp.swapaxes(up, 1, 2), jnp.swapaxes(down, 1, 2), combined
+    return jnp.swapaxes(gate, 1, 2), jnp.swapaxes(up, 1, 2), jnp.swapaxes(down, 1, 2), jnp.transpose(out)
 
 
 def solution(mesh):

time: 176 us -> 166 us (0.943)
  Pallas kernels: 160 us -> 156 us
  other arithmetic: 4.39 us -> 0.81 us
  local copies, waits for them, and re-layouts: 10.5 us -> 7.69 us
    pallas_call x1, Pallas kernels: 160 us -> 156 us  [whole_call(): pl.pallas_call(whole, out_shape=(served, served, served, jax.ShapeDtypeSt...]
    unnamed x9 -> x10, local copies, waits for them, and re-layouts: 6.66 us -> 7.1 us
where the time goes in v3:
time: 166 us; the launch traced here: 165 us
  Pallas kernels  156 us (94%)
  local copies, waits for them, and re-layouts  7.69 us (5%)
    pallas_call x1, Pallas kernels, whole_call(): pl.pallas_call(whole, out_shape=(served, served, served, jax.ShapeDtypeSt...  156 us
    unnamed x10, local copies, waits for them, and re-layouts  7.1 us

profile of v3, /device:TPU:1, one launch (start us, length us, event | category | flops | bytes accessed | tf_op | source)
XLA Modules:
  0.0 165.4 jit_solution(7375322260062906689)
XLA Ops:
  0.6 0.8 pad_maximum_fusion
  1.4 0.6 broadcast_in_dim.2.gain
  2.0 156.3 %whole.1 = (bf16[2,224,2048]{2,1,0:T(8,128)(2,1)}, bf16[2,224,2048]{2,1,0:T(8,128)(2,1)}, bf16[2,224,2048]{2,1,0:T(8,128)(2,1)}, bf16[64,512]{1,0:T(8,128)(2,1)}) custom-call(f32[4,2,64,1792]{3,2,1,0:T(8,128)} %bitcast.10, f32[4,2,64,1792]{3,2,1,0:T(8,128)} %bitcast.11, f32[4,2,64,1792]{3,2,1,0:T(8,128)} %bitcast.12, f32[8,128]{1,0:T(8,128)} %broadcast_in_dim.2.gain, ...), custom_call_target="tpu_custom_call" | custom-call | tf_op jit(solution)/shard_map/whole/pallas_call | solution.py:423
  158.3 0.0 copy-start.1
  158.3 3.1 %copy.15 = bf16[2,2048,224]{1,2,0:T(8,128)(2,1)} copy(bf16[2,2048,224]{1,2,0:T(8,128)(2,1)} %bitcast.15) | data formatting | bytes 3670016
  161.4 0.0 copy-done.1
  161.4 0.0 copy-start
  161.4 1.2 copy.16
  162.6 0.9 copy-done
  163.5 0.0 copy-start.2
  163.5 1.2 copy.17
  164.8 0.0 copy-done.2
  164.8 0.6 copy.18
Async XLA Ops:
  158.3 3.1 %copy-start.1 = (bf16[2,224,2048]{2,1,0:T(8,128)(2,1)S(1)}, bf16[2,224,2048]{2,1,0:T(8,128)(2,1)}, u32[]{:S(2)}) copy-start(bf16[2,224,2048]{2,1,0:T(8,128)(2,1)} %get-tuple-element.9) | copy-start | bytes 5505028
  161.4 2.2 %copy-start = (bf16[2,224,2048]{2,1,0:T(8,128)(2,1)S(1)}, bf16[2,224,2048]{2,1,0:T(8,128)(2,1)}, u32[]{:S(2)}) copy-start(bf16[2,224,2048]{2,1,0:T(8,128)(2,1)} %get-tuple-element.10) | copy-start | bytes 5505028
  163.5 1.2 copy-start.2

commit v4 on v3

--- a/solution.py
+++ b/solution.py
@@ -12,9 +12,10 @@
 EPSILON = 1e-06
 FS = ("z", "y", "c")
 HOPS = (1, 3, 2)
+GATHER_AT = 1
 STEPS = HOPS + (0,)
 ROWS = ((0, 96), (96, 80), (176, 80))
-HALVES = ((0, 128), (128, 128))
+ROUTES = ((0, 64, "xyz"), (64, 128, "xzy"), (192, 64, "yzx"))
 CHUNKS = 12
 
 
@@ -44,7 +45,7 @@
           wide, acts, give, near, held, one0, one1, one2, add0, add1, add2,
           two0, two1, two2, sum0, sum1, sum2, three0, three1, three2, last, turned,
           ls, ps, pr, credit, xs, xr, zs, zr, ys, yr, hs, hr, ns, nr, ws, wr,
-          g0s, g0r, gs, gr, hops, hopr, cs, cr, os, ds, dr, f0s, f0r, fs, fr, ss, sr, ts, tr, es, er):
+          gs, gr, hops, hopr, cs, cr, os, ds, dr, f0s, f0r, fs, fr, ss, sr, ts, tr, es, er):
     masters = (gate, up, down)
     outs = (gate_out, up_out, down_out)
     x, y, z, c = (lax.axis_index(a) for a in ("x", "y", "z", "c"))
@@ -93,56 +94,60 @@
         expert = lax.broadcasted_iota(jnp.int32, (8, 512), 0) + 2 * to
         shares[to] = jnp.where(ids[0:1] == expert, w0, 0.0) + jnp.where(ids[1:2] == expert, w1, 0.0)
     near_shares[x] = shares[x]
-    swap(1)
-
     halves.wait_recv()
     tokens[z, y, x, c] = jnp.transpose(chip[...].astype(jnp.float32)).astype(jnp.bfloat16)
     flows = {}
+    spot = {"x": x, "y": y, "z": z}
 
     def arrived(group):
         for cp in group:
             cp.wait_recv()
 
-    def spot(axis, at, rows):
-        return (at if axis == "z" else slice(None), at if axis == "y" else slice(None), slice(None), c, rows)
-
-    own = tokens.at[z, y, x, c]
-    flows["x"] = [
-        start(push(own, own, g0s.at[i], g0r.at[i], {"x": along("x", h)})) for i, h in enumerate(HOPS)
-    ]
+    def part(l, s, at=None, half=None):
+        first, count, order = ROUTES[l]
+        if half is not None:
+            first, count = first + half * (count // 2), count // 2
+        where = dict(spot, **(at or {}))
+        index = tuple(slice(None) if a in order[:s] else where[a] for a in "zyx")
+        return tokens.at[index + (c, pl.ds(first, count))]
+
+    def gather(l, s):
+        axis = ROUTES[l][2][s]
+        flows["g", l, s] = [
+            start(push(part(l, s), part(l, s), gs.at[l, s, i], gr.at[l, s, i], {axis: along(axis, h)}))
+            for i, h in enumerate(HOPS)
+        ]
+
+    for l in range(3):
+        gather(l, 0)
     share_swaps = []
     for i, h in enumerate(HOPS):
         peer = along("x", h)
         share_swaps.append(start(push(shares.at[peer], near_shares.at[x], ws.at[i], wr.at[i], {"x": peer})))
+    swap(1)
     gain_swap.wait_recv()
     gains[...] = jnp.where((lane < 64) == (c == 0), doubled, gains[...])
-    arrived(flows["x"])
-    for l, axis in enumerate(("y", "z")):
-        part = tokens.at[z, y, slice(None), c, pl.ds(*HALVES[l])]
-        flows["g", l] = [
-            start(push(part, part, gs.at[l, i], gr.at[l, i], {axis: along(axis, h)}))
-            for i, h in enumerate(HOPS)
-        ]
 
     def spread_out(l):
-        axis = ("z", "y")[l]
-        arrived(flows["g", l])
-        part = tokens.at[spot(axis, lax.axis_index(axis), pl.ds(*HALVES[l]))]
+        axis = ROUTES[l][2][2]
         flows["n", l] = [
-            start(push(part, part, hops.at[l, i], hopr.at[l, i], {axis: along(axis, h)}))
+            start(push(part(l, 2), part(l, 2), hops.at[l, i], hopr.at[l, i], {axis: along(axis, h)}))
             for i, h in enumerate((1, 3))
         ]
 
     def pass_on(l):
-        axis = ("z", "y")[l]
-        first, count = HALVES[l]
+        axis = ROUTES[l][2][2]
         flows["p", l] = []
         for i, h in enumerate((1, 3)):
             flows["n", l][i].wait_recv()
-            rows = pl.ds(first + i * (count // 2), count // 2)
-            part = tokens.at[spot(axis, along(axis, 4 - h), rows)]
-            cp = push(part, part, hops.at[l, 2 + i], hopr.at[l, 2 + i], {axis: along(axis, h)})
+            block = part(l, 2, {axis: along(axis, 4 - h)}, i)
+            cp = push(block, block, hops.at[l, 2 + i], hopr.at[l, 2 + i], {axis: along(axis, h)})
             flows["p", l].append(start(cp))
+            if axis == "x":
+                to_core(3 + i, part(l, 2, {axis: along(axis, 4 - h)}))
+
+    def to_core(n, block):
+        flows["c", n] = [start(push(block, block, cs.at[n], cr.at[n], other))]
 
     def pack_one(m, to):
         for t in range(14):
@@ -228,6 +233,10 @@
         pack_one(0, along("x", h))
         if i < 3:
             x_send(0, i)
+        if i == GATHER_AT:
+            for l in range(3):
+                arrived(flows["g", l, 0])
+                gather(l, 1)
     for k in range(1, 4):
         for i in range(3):
             x_send(k, i)
@@ -235,23 +244,23 @@
     fetch(2)
     for k in range(4):
         x_keep(k)
-    spread_out(0)
-    spread_out(1)
+    z_step(0)
+    for l in range(2):
+        arrived(flows["g", l, 1])
+        spread_out(l)
     pl.semaphore_wait(credit, 1)
     swap(2)
     pack(1)
     x_steps(1)
-    z_step(0)
+    arrived(flows["g", 2, 1])
+    to_core(2, part(2, 2))
+    z_step(1)
     pack(2)
     x_steps(2)
+    spread_out(2)
     arrived(share_swaps)
     for b in range(4):
         share_cols[pl.ds(512 * b, 512), 0:8] = jnp.transpose(near_shares[b])
-
-    def core_step(l):
-        arrived(flows["p", l])
-        part = tokens.at[:, :, :, c, pl.ds(*HALVES[l])]
-        flows["c", l] = [start(push(part, part, cs.at[l], cr.at[l], other))]
 
     stores = []
 
@@ -260,8 +269,8 @@
         cp.start()
         stores.append(cp)
 
-    def act_tile(t, carry):
-        xb, ch = t // 2, lax.rem(t, 2)
+    def act_tile(xb, ch):
+        t = xb * 2 + ch
         total = jnp.zeros((256, 128), jnp.float32)
         for q in range(16):
             block = tokens[q // 4, q % 4, xb, ch]
@@ -276,30 +285,45 @@
             up_pre = lax.dot_general(wide[...], served[1, e], dims, preferred_element_type=jnp.float32) * inv
             act = gate_pre / (1.0 + jnp.exp(-gate_pre)) * up_pre
             acts[e, rows] = (act * share_cols[rows, e : e + 1]).astype(jnp.bfloat16)
-        return carry
-
-    for k in range(1, 10):
-        z_step(k)
-        y_step(k - 1)
-        if k == 2:
+
+    def act_block(hop):
+        def one(ch, carry):
+            act_tile(along("x", hop), ch)
+            return carry
+
+        lax.fori_loop(0, 2, one, 0)
+
+    for k in range(9):
+        if k < 8:
+            z_step(k + 2)
+        if k == 1:
             pass_on(0)
             pass_on(1)
-        if k in (6, 7):
-            core_step(k - 6)
-    for l in range(2):
-        arrived(flows["c", l])
+        if k in (5, 6):
+            arrived(flows["p", k - 5])
+            to_core(k - 5, part(k - 5, 3))
+        y_step(k)
+    z_step(10)
+    z_step(11)
+    pass_on(2)
+    y_step(9)
     for k in range(8):
         arrived(flows["y", k])
     store(0)
     store(1)
-    lax.fori_loop(0, 3, act_tile, 0)
-    z_step(10)
-    y_step(9)
-    lax.fori_loop(3, 6, act_tile, 0)
-    z_step(11)
+    for n in range(3):
+        arrived(flows["c", n])
+    act_block(0)
+    arrived(flows["p", 2])
+    to_core(5, part(2, 2, {"x": along("x", 2)}))
     y_step(10)
-    lax.fori_loop(6, 8, act_tile, 0)
+    arrived(flows["c", 3])
+    act_block(3)
+    arrived(flows["c", 4])
     y_step(11)
+    act_block(1)
+    arrived(flows["c", 5])
+    act_block(2)
     for k in range(8, 12):
         arrived(flows["y", k])
     store(2)
@@ -442,10 +466,9 @@
         + [dma((CHUNKS, 4))] * 2
         + [dma] * 4
         + [dma((3,))] * 2
-        + [dma((3,))] * 2
-        + [dma((2, 3))] * 2
-        + [dma((2, 4))] * 2
-        + [dma((2,))] * 2
+        + [dma((3, 2, 3))] * 2
+        + [dma((3, 4))] * 2
+        + [dma((6,))] * 2
         + [dma((3,))]
         + [dma((4,))] * 2
         + [dma((3,))] * 2

time: 166 us -> 152 us (0.916)
  Pallas kernels: 156 us -> 143 us
    pallas_call x1, Pallas kernels: 156 us -> 143 us  [whole_call(): pl.pallas_call(whole, out_shape=(served, served, served, jax.ShapeDtypeSt...]
where the time goes in v4:
time: 152 us
  Pallas kernels  143 us (94%)
  local copies, waits for them, and re-layouts  7.69 us (5%)
    pallas_call x1, Pallas kernels, whole_call(): pl.pallas_call(whole, out_shape=(served, served, served, jax.ShapeDtypeSt...  143 us
    unnamed x10, local copies, waits for them, and re-layouts  7.1 us

profile of v4, /device:TPU:1, one launch (start us, length us, event | category | flops | bytes accessed | tf_op | source)
XLA Modules:
  0.0 152.0 jit_solution(9617904729858525664)
XLA Ops:
  0.6 0.8 pad_maximum_fusion
  1.4 0.6 broadcast_in_dim.2.gain
  2.0 142.8 %whole.1 = (bf16[2,224,2048]{2,1,0:T(8,128)(2,1)}, bf16[2,224,2048]{2,1,0:T(8,128)(2,1)}, bf16[2,224,2048]{2,1,0:T(8,128)(2,1)}, bf16[64,512]{1,0:T(8,128)(2,1)}) custom-call(f32[4,2,64,1792]{3,2,1,0:T(8,128)} %bitcast.10, f32[4,2,64,1792]{3,2,1,0:T(8,128)} %bitcast.11, f32[4,2,64,1792]{3,2,1,0:T(8,128)} %bitcast.12, f32[8,128]{1,0:T(8,128)} %broadcast_in_dim.2.gain, ...), custom_call_target="tpu_custom_call" | custom-call | tf_op jit(solution)/shard_map/whole/pallas_call | solution.py:447
  144.9 0.0 copy-start.1
  144.9 3.1 %copy.15 = bf16[2,2048,224]{1,2,0:T(8,128)(2,1)} copy(bf16[2,2048,224]{1,2,0:T(8,128)(2,1)} %bitcast.15) | data formatting | bytes 3670016
  148.0 0.0 copy-done.1
  148.0 0.0 copy-start
  148.0 1.2 copy.16
  149.2 0.9 copy-done
  150.1 0.0 copy-start.2
  150.1 1.2 copy.17
  151.4 0.0 copy-done.2
  151.4 0.6 copy.18
Async XLA Ops:
  144.9 3.1 %copy-start.1 = (bf16[2,224,2048]{2,1,0:T(8,128)(2,1)S(1)}, bf16[2,224,2048]{2,1,0:T(8,128)(2,1)}, u32[]{:S(2)}) copy-start(bf16[2,224,2048]{2,1,0:T(8,128)(2,1)} %get-tuple-element.9) | copy-start | bytes 5505028
  148.0 2.2 %copy-start = (bf16[2,224,2048]{2,1,0:T(8,128)(2,1)S(1)}, bf16[2,224,2048]{2,1,0:T(8,128)(2,1)}, u32[]{:S(2)}) copy-start(bf16[2,224,2048]{2,1,0:T(8,128)(2,1)} %get-tuple-element.10) | copy-start | bytes 5505028
  150.1 1.2 copy-start.2

commit v5 on v4

--- a/solution.py
+++ b/solution.py
@@ -12,10 +12,9 @@
 EPSILON = 1e-06
 FS = ("z", "y", "c")
 HOPS = (1, 3, 2)
-GATHER_AT = 1
 STEPS = HOPS + (0,)
 ROWS = ((0, 96), (96, 80), (176, 80))
-ROUTES = ((0, 64, "xyz"), (64, 128, "xzy"), (192, 64, "yzx"))
+ROUTES = ((0, 64, "xyz"), (64, 96, "xzy"), (160, 96, "zyx"))
 CHUNKS = 12
 
 
@@ -41,11 +40,11 @@
 
 def whole(gate, up, down, gain, hidden, ids, logits,
           gate_out, up_out, down_out, out,
-          raw, gains, sent, over_x, over_z, served, tokens, chip, shares, near_shares, share_cols,
+          raw, doubled, gains, sent, over_x, over_z, served, tokens, chip, shares, near_shares, share_cols,
           wide, acts, give, near, held, one0, one1, one2, add0, add1, add2,
           two0, two1, two2, sum0, sum1, sum2, three0, three1, three2, last, turned,
           ls, ps, pr, credit, xs, xr, zs, zr, ys, yr, hs, hr, ns, nr, ws, wr,
-          gs, gr, hops, hopr, cs, cr, os, ds, dr, f0s, f0r, fs, fr, ss, sr, ts, tr, es, er):
+          gs, gr, hops, hopr, cs, cr, os, ds, dr, fs, fr, ss, sr, ts, tr, es, er):
     masters = (gate, up, down)
     outs = (gate_out, up_out, down_out)
     x, y, z, c = (lax.axis_index(a) for a in ("x", "y", "z", "c"))
@@ -57,22 +56,27 @@
         sends.append(cp)
         return cp
 
+    def bulk(ref, send, recv):
+        return push(ref, ref, send, recv, other)
+
     mine = pl.ds(pl.multiple_of(c * 64, 64), 64)
-    loads, pushes = {}, {}
+    def slot(m, i):
+        return i if m == 0 else 3 + m
 
     def fetch(m):
         for i, h in enumerate(STEPS):
             to = along("x", h)
-            cp = pltpu.make_async_copy(masters[m].at[to, c], raw.at[m % 2, to, mine], ls.at[m, i])
-            cp.start()
-            loads[m, i] = cp
+            pltpu.make_async_copy(masters[m].at[to, c], raw.at[m % 2, to, mine], ls.at[slot(m, i)]).start()
 
     def swap(m):
         for i, h in enumerate(STEPS):
             to = along("x", h)
-            pushes[m, i] = start(
-                push(masters[m].at[to, 1 - c], raw.at[m % 2, to, mine], ps.at[m, i], pr.at[m, i], other)
-            )
+            push(masters[m].at[to, 1 - c], raw.at[m % 2, to, mine], ps, pr.at[slot(m, i)], other).start()
+
+    def loaded(m, i):
+        block = raw.at[0, 0, mine] if m == 0 else raw.at[0, :, mine]
+        pltpu.make_async_copy(block, block, ls.at[slot(m, i)]).wait()
+        bulk(block, ps, pr.at[slot(m, i)]).wait_recv()
 
     fetch(0)
     fetch(1)
@@ -80,10 +84,11 @@
     far_half = pl.ds(pl.multiple_of((1 - c) * 256, 256), 256)
     chip[mine] = hidden[:, half]
     lane = lax.broadcasted_iota(jnp.int32, (8, 128), 1)
-    doubled = jnp.broadcast_to(gain[...], (8, 128))
+    row = jnp.broadcast_to(gain[...], (8, 64))
+    doubled[...] = jnp.concatenate([row, row], axis=1)
     greet()
     halves = start(push(hidden.at[:, far_half], chip.at[mine], hs, hr, other))
-    gain_swap = start(push(gain, gains, ns, nr, other))
+    gain_swap = start(push(doubled, gains, ns, nr, other))
     swap(0)
 
     l0, l1 = logits[0:1], logits[1:2]
@@ -126,7 +131,7 @@
         share_swaps.append(start(push(shares.at[peer], near_shares.at[x], ws.at[i], wr.at[i], {"x": peer})))
     swap(1)
     gain_swap.wait_recv()
-    gains[...] = jnp.where((lane < 64) == (c == 0), doubled, gains[...])
+    gains[...] = jnp.where((lane < 64) == (c == 0), doubled[...], gains[...])
 
     def spread_out(l):
         axis = ROUTES[l][2][2]
@@ -164,9 +169,7 @@
                 at += n
 
     def pack(m):
-        for i in range(4):
-            loads[m, i].wait()
-            pushes[m, i].wait_recv()
+        loaded(m, 0)
 
         def one(to, carry):
             pack_one(m, to)
@@ -181,7 +184,7 @@
         m, hh, rc = split(k)
         peer = along("x", HOPS[i])
         src = sent.at[m, peer, :, lax.rem(c + rc, 2), hh]
-        flows["x", k].append(start(push(src, over_x.at[k, x], xs.at[k, i], xr.at[k, i], {"x": peer})))
+        push(src, over_x.at[k, x], xs, xr.at[k], {"x": peer}).start()
 
     def x_keep(k):
         m, hh, rc = split(k)
@@ -189,19 +192,16 @@
 
     def x_steps(m):
         for k in range(4 * m, 4 * m + 4):
-            flows["x", k] = []
             for i in range(3):
                 x_send(k, i)
         for k in range(4 * m, 4 * m + 4):
             x_keep(k)
 
     def z_step(k):
-        arrived(flows["x", k])
-        flows["z", k] = [
-            start(push(over_x.at[k, along("z", h)], over_z.at[k, z], zs.at[k, i], zr.at[k, i],
-                       {"z": along("z", h)}))
-            for i, h in enumerate(HOPS)
-        ]
+        bulk(over_x.at[k, 0:3], xs, xr.at[k]).wait_recv()
+        for h in HOPS:
+            peer = along("z", h)
+            push(over_x.at[k, peer], over_z.at[k, z], zs, zr.at[k], {"z": peer}).start()
         over_z[k, z] = over_x[k, z]
 
     def lanes(zz):
@@ -209,37 +209,32 @@
 
     def y_step(k):
         m, hh, rc = split(k)
-        arrived(flows["z", k])
+        bulk(over_z.at[k, 0:3], zs, zr.at[k]).wait_recv()
         rows = pl.ds(hh * 112, 112)
-        flows["y", k] = []
-        for i, h in enumerate(STEPS if rc else HOPS):
+        for h in STEPS if rc else HOPS:
             py = along("y", h)
             peer = {"y": py, "c": lax.rem(c + rc, 2)}
             for zz in range(4):
-                push(over_z.at[k, zz, py], served.at[m, c, rows, lanes(zz)],
-                     ys.at[k, i], yr.at[k, i], peer).start()
-            cp = push(over_z.at[k, :, 0], over_z.at[k, :, 0], ys.at[k, i], yr.at[k, i], peer)
-            flows["y", k].append(cp)
-            sends.append(cp)
+                push(over_z.at[k, zz, py], served.at[m, c, rows, lanes(zz)], ys.at[rc], yr.at[k], peer).start()
         if rc == 0:
             for zz in range(4):
                 served[m, c, rows, lanes(zz)] = over_z[k, zz, y]
 
-    for k in range(4):
-        flows["x", k] = []
+    def y_landed(k):
+        rc = k % 2
+        bulk(over_z.at[k, 0 : 3 + rc], ys.at[rc], yr.at[k]).wait_recv()
+
     for i, h in enumerate(STEPS):
-        loads[0, i].wait()
-        pushes[0, i].wait_recv()
+        loaded(0, i)
         pack_one(0, along("x", h))
         if i < 3:
             x_send(0, i)
-        if i == GATHER_AT:
-            for l in range(3):
-                arrived(flows["g", l, 0])
-                gather(l, 1)
     for k in range(1, 4):
         for i in range(3):
             x_send(k, i)
+    for l in range(3):
+        arrived(flows["g", l, 0])
+        gather(l, 1)
     pl.semaphore_signal(credit, inc=1, device_id=other, device_id_type=MESH)
     fetch(2)
     for k in range(4):
@@ -305,27 +300,27 @@
         y_step(k)
     z_step(10)
     z_step(11)
-    pass_on(2)
     y_step(9)
     for k in range(8):
-        arrived(flows["y", k])
+        y_landed(k)
     store(0)
     store(1)
     for n in range(3):
         arrived(flows["c", n])
     act_block(0)
+    y_step(10)
+    pass_on(2)
+    y_step(11)
+    arrived(flows["c", 4])
+    act_block(1)
     arrived(flows["p", 2])
     to_core(5, part(2, 2, {"x": along("x", 2)}))
-    y_step(10)
     arrived(flows["c", 3])
     act_block(3)
-    arrived(flows["c", 4])
-    y_step(11)
-    act_block(1)
     arrived(flows["c", 5])
     act_block(2)
     for k in range(8, 12):
-        arrived(flows["y", k])
+        y_landed(k)
     store(2)
 
     def down_part(t, n):
@@ -343,7 +338,6 @@
                 give[i, n, b] = v[:, 128 * b : 128 * b + 128].astype(jnp.bfloat16)
         given.append(start(push(give.at[i], near.at[i], ds.at[i], dr.at[i], other)))
     r0, r1, r2 = (pl.ds(*r) for r in ROWS)
-    first = ([], [], [])
     every = slice(None)
     for i, h in enumerate(STEPS):
         t = along("x", h) * 2 + c
@@ -354,17 +348,11 @@
                 total = v[:, 128 * b : 128 * b + 128] + near[i, n, b].astype(jnp.float32)
                 held[n, b, i] = total.astype(jnp.bfloat16)
         if i < 3:
-            first[0].append(
-                start(push(held.at[every, every, i, r0], one0.at[i], f0s.at[i], f0r.at[i], {"x": along("x", h)}))
-            )
+            push(held.at[every, every, i, r0], one0.at[i], fs.at[0], fr.at[0], {"x": along("x", h)}).start()
         for j, g in enumerate(HOPS):
             py, pz = along("y", g), along("z", g)
-            first[1].append(
-                start(push(held.at[every, py, i, r1], one1.at[j, :, i], fs.at[0, i, j], fr.at[0, i, j], {"y": py}))
-            )
-            first[2].append(
-                start(push(held.at[pz, every, i, r2], one2.at[j, :, i], fs.at[1, i, j], fr.at[1, i, j], {"z": pz}))
-            )
+            push(held.at[every, py, i, r1], one1.at[j, :, i], fs.at[1], fr.at[1], {"y": py}).start()
+            push(held.at[pz, every, i, r2], one2.at[j, :, i], fs.at[2], fr.at[2], {"z": pz}).start()
 
     def summed(base, terms):
         v = base.astype(jnp.float32)
@@ -372,61 +360,60 @@
             v = v + term.astype(jnp.float32)
         return v
 
-    def add_first(l, one, add, base):
-        arrived(first[l])
+    ones, twos, threes = (one0, one1, one2), (two0, two1, two2), (three0, three1, three2)
+    adds, sums = (add0, add1, add2), (sum0, sum1, sum2)
+    turns = (("y", "z"), ("z", "x"), ("x", "y"))
+
+    def add_first(l, base):
+        bulk(ones[l], fs.at[l], fr.at[l]).wait_recv()
 
         def body(n, carry):
             a, b = n // 4, lax.rem(n, 4)
-            add[a, b] = summed(base(a, b), [one[j, a, b] for j in range(3)]).astype(jnp.bfloat16)
+            adds[l][a, b] = summed(base(a, b), [ones[l][j, a, b] for j in range(3)]).astype(jnp.bfloat16)
             return carry
 
         lax.fori_loop(0, 16, body, 0)
 
-    second, third = [], []
-    add_first(0, one0, add0, lambda a, b: held[a, b, 3, r0])
-    second.append([
-        start(push(add0.at[:, along("y", h)], two0.at[j], ss.at[0, j], sr.at[0, j], {"y": along("y", h)}))
-        for j, h in enumerate(HOPS)
-    ])
-    add_first(1, one1, add1, lambda a, b: held[a, y, b, r1])
-    second.append([
-        start(push(add1.at[along("z", h)], two1.at[j], ss.at[1, j], sr.at[1, j], {"z": along("z", h)}))
-        for j, h in enumerate(HOPS)
-    ])
-    add_first(2, one2, add2, lambda a, b: held[z, a, b, r2])
-    second.append([
-        start(push(add2.at[:, j], two2.at[j], ss.at[2, j], sr.at[2, j], {"x": along("x", h)}))
-        for j, h in enumerate(HOPS)
-    ])
-
-    def add_second(l, two, into, base):
-        arrived(second[l])
+    def add_second(l, base):
+        bulk(twos[l], ss.at[l], sr.at[l]).wait_recv()
         for a in range(4):
-            into[a] = summed(base(a), [two[j, a] for j in range(3)]).astype(jnp.bfloat16)
-
-    add_second(0, two0, sum0, lambda a: add0[a, y])
-    third.append([
-        start(push(sum0.at[along("z", h)], three0.at[j], ts.at[0, j], tr.at[0, j], {"z": along("z", h)}))
-        for j, h in enumerate(HOPS)
-    ])
-    add_second(1, two1, sum1, lambda a: add1[z, a])
-    third.append([
-        start(push(sum1.at[j], three1.at[j], ts.at[1, j], tr.at[1, j], {"x": along("x", h)}))
-        for j, h in enumerate(HOPS)
-    ])
-    add_second(2, two2, sum2, lambda a: add2[a, 3])
-    third.append([
-        start(push(sum2.at[along("y", h)], three2.at[j], ts.at[2, j], tr.at[2, j], {"y": along("y", h)}))
-        for j, h in enumerate(HOPS)
-    ])
-    for l, (three, base) in enumerate(((three0, sum0[z]), (three1, sum1[3]), (three2, sum2[y]))):
-        arrived(third[l])
-        last[pl.ds(*ROWS[l])] = summed(base, [three[j] for j in range(3)]).astype(jnp.bfloat16)
+            sums[l][a] = summed(base(a), [twos[l][j, a] for j in range(3)]).astype(jnp.bfloat16)
+
+    def send_on(l, s, pick, dst, send, recv):
+        axis = turns[l][s]
+        for j, h in enumerate(HOPS):
+            peer = along(axis, h)
+            push(pick(j, peer), dst.at[j], send.at[l], recv.at[l], {axis: peer}).start()
+
+    bases = (lambda a, b: held[a, b, 3, r0], lambda a, b: held[a, y, b, r1], lambda a, b: held[z, a, b, r2])
+    picks = (lambda j, p: add0.at[:, p], lambda j, p: add1.at[p], lambda j, p: add2.at[:, j])
+    for l in (1, 2, 0):
+        add_first(l, bases[l])
+        send_on(l, 0, picks[l], twos[l], ss, sr)
+    bases = (lambda a: add0[a, y], lambda a: add1[z, a], lambda a: add2[a, 3])
+    picks = (lambda j, p: sum0.at[p], lambda j, p: sum1.at[j], lambda j, p: sum2.at[p])
+    for l in (1, 2, 0):
+        add_second(l, bases[l])
+        send_on(l, 1, picks[l], threes[l], ts, tr)
+    bases = (lambda: sum0[z], lambda: sum1[3], lambda: sum2[y])
+    for l in (1, 2, 0):
+        bulk(threes[l], ts.at[l], tr.at[l]).wait_recv()
+        total = summed(bases[l](), [threes[l][j] for j in range(3)])
+        last[pl.ds(*ROWS[l])] = total.astype(jnp.bfloat16)
     turned[...] = jnp.transpose(last[...].astype(jnp.float32)).astype(jnp.bfloat16)
     rest = turned.at[pl.ds(pl.multiple_of((1 - c) * 64, 64), 64)]
     final = start(push(rest, out.at[:, half], es, er, other))
     out[:, half] = turned[mine]
     final.wait_recv()
+    bulk(raw.at[:, 0:3], ps, pr.at[0]).wait_send()
+    bulk(over_x.at[:, 0:3], xs, xr.at[0]).wait_send()
+    bulk(over_z.at[:, 0:3], zs, zr.at[0]).wait_send()
+    for rc in range(2):
+        bulk(over_z.at[0:6, 0 : 3 + rc], ys.at[rc], yr.at[0]).wait_send()
+    for l in range(3):
+        bulk(ones[l], fs.at[l], fr.at[l]).wait_send()
+        bulk(twos[l], ss.at[l], sr.at[l]).wait_send()
+        bulk(threes[l], ts.at[l], tr.at[l]).wait_send()
     for cp in sends:
         cp.wait_send()
     for cp in stores:
@@ -449,7 +436,7 @@
         out_shape=(served, served, served, jax.ShapeDtypeStruct((64, 512), bf16)),
         in_specs=[any_space] * 3 + [vmem] * 4,
         out_specs=(any_space,) * 3 + (vmem,),
-        scratch_shapes=[pltpu.VMEM((2, 4, 128, 1792), f32), pltpu.VMEM((8, 128), f32)]
+        scratch_shapes=[pltpu.VMEM((2, 4, 128, 1792), f32)] + [pltpu.VMEM((8, 128), f32)] * 2
         + buffers((3, 4, 4, 2, 2, 112, 128), (CHUNKS, 4, 4, 112, 128), (CHUNKS, 4, 4, 112, 128),
                   (3, 2, 224, 2048), (4, 4, 4, 2, 256, 128), (128, 256))
         + [pltpu.VMEM((4, 8, 512), f32)] * 2
@@ -461,9 +448,8 @@
         + buffers(*[(4, n, 128) for n in sizes])
         + buffers(*[(3, n, 128) for n in sizes])
         + buffers((256, 128), (128, 256))
-        + [dma((3, 4)), dma((3, 4)), dma((3, 4)), pltpu.SemaphoreType.REGULAR]
-        + [dma((CHUNKS, 3))] * 4
-        + [dma((CHUNKS, 4))] * 2
+        + [dma((6,)), dma, dma((6,)), pltpu.SemaphoreType.REGULAR]
+        + [dma, dma((CHUNKS,)), dma, dma((CHUNKS,)), dma((2,)), dma((CHUNKS,))]
         + [dma] * 4
         + [dma((3,))] * 2
         + [dma((3, 2, 3))] * 2
@@ -471,9 +457,7 @@
         + [dma((6,))] * 2
         + [dma((3,))]
         + [dma((4,))] * 2
-        + [dma((3,))] * 2
-        + [dma((2, 4, 3))] * 2
-        + [dma((3, 3))] * 4
+        + [dma((3,))] * 6
         + [dma] * 2,
         compiler_params=pltpu.CompilerParams(
             collective_id=0, has_side_effects=True, vmem_limit_bytes=67043328
@@ -482,12 +466,48 @@
     )(gate, up, down, gain, hidden, ids, logits)
 
 
+def deliver(*refs):
+    sources, results, held, in_sem, out_sem = refs[:4], refs[4:8], refs[8:12], refs[12], refs[13]
+
+    def view(ref, n, k):
+        return ref.at[k // 2, pl.ds(112 * (k % 2), 112)] if n < 3 else ref
+
+    steps = [(n, k) for n in range(4) for k in range(4 if n < 3 else 1)]
+    loads = [
+        pltpu.make_async_copy(view(sources[n], n, k), view(held[n], n, k), in_sem.at[4 * n + k]) for n, k in steps
+    ]
+    stores = [
+        pltpu.make_async_copy(view(held[n], n, k), view(results[n], n, k), out_sem.at[4 * n + k]) for n, k in steps
+    ]
+    for cp in loads:
+        cp.start()
+    for load, store in zip(loads, stores):
+        load.wait()
+        store.start()
+    for cp in stores:
+        cp.wait()
+
+
+def deliver_call(*results):
+    any_space = pl.BlockSpec(memory_space=pl.ANY)
+    return pl.pallas_call(
+        deliver,
+        out_shape=tuple(jax.ShapeDtypeStruct(r.shape, r.dtype) for r in results),
+        in_specs=[any_space] * 4,
+        out_specs=(any_space,) * 4,
+        scratch_shapes=[pltpu.VMEM(r.shape, r.dtype) for r in results]
+        + [pltpu.SemaphoreType.DMA((13,))] * 2,
+        name="deliver",
+    )(*results)
+
+
 def per_device(hidden, norm_gain, gate_master, up_master, down_master, expert_ids, route_logits):
-    gain = jnp.broadcast_to(jnp.concatenate([norm_gain, norm_gain])[None, :], (8, 128))
+    gain = norm_gain.reshape(1, 64)
     masters = [m.reshape(4, 2, 64, 1792) for m in (gate_master, up_master, down_master)]
-    gate, up, down, out = whole_call(
+    results = whole_call(
         *masters, gain, jnp.transpose(hidden), jnp.transpose(expert_ids), jnp.transpose(route_logits)
     )
+    gate, up, down, out = deliver_call(*results)
     return jnp.swapaxes(gate, 1, 2), jnp.swapaxes(up, 1, 2), jnp.swapaxes(down, 1, 2), jnp.transpose(out)
 
 

time: 152 us -> 144 us (0.947)
  local copies, waits for them, and re-layouts: 7.69 us -> 0 us
    unnamed x10 -> x0, local copies, waits for them, and re-layouts: 7.1 us -> none
    pallas_call x0 -> x1, Pallas kernels: none -> 5.05 us  [deliver_call(): pl.pallas_call(deliver, out_shape=tuple((jax.ShapeDtypeStruct(r.shape, r....]
    pallas_call x1, Pallas kernels: 143 us -> 138 us  [whole_call(): pl.pallas_call(whole, out_shape=(served, served, served, jax.ShapeDtypeSt...]
where the time goes in v5:
time: 144 us
  Pallas kernels  143 us (99%)
    pallas_call x1, Pallas kernels, whole_call(): pl.pallas_call(whole, out_shape=(served, served, served, jax.ShapeDtypeSt...  138 us
    pallas_call x1, Pallas kernels, deliver_call(): pl.pallas_call(deliver, out_shape=tuple((jax.ShapeDtypeStruct(r.shape, r....  5.05 us

profile of v5, /device:TPU:1, one launch (start us, length us, event | category | flops | bytes accessed | tf_op | source)
XLA Modules:
  0.0 143.7 jit_solution(11822246503597519301)
XLA Ops:
  0.6 138.0 %whole.1 = (bf16[2,224,2048]{2,1,0:T(8,128)(2,1)}, bf16[2,224,2048]{2,1,0:T(8,128)(2,1)}, bf16[2,224,2048]{2,1,0:T(8,128)(2,1)}, bf16[64,512]{1,0:T(8,128)(2,1)}) custom-call(f32[4,2,64,1792]{3,2,1,0:T(8,128)} %bitcast.11, f32[4,2,64,1792]{3,2,1,0:T(8,128)} %bitcast.12, f32[4,2,64,1792]{3,2,1,0:T(8,128)} %bitcast.13, f32[1,64]{1,0:T(1,128)} %bitcast.17, ...), custom_call_target="tpu_custom_call" | custom-call | tf_op jit(solution)/shard_map/whole/pallas_call | solution.py:434
  138.6 5.1 %deliver.1 = (bf16[2,224,2048]{2,1,0:T(8,128)(2,1)}, bf16[2,224,2048]{2,1,0:T(8,128)(2,1)}, bf16[2,224,2048]{2,1,0:T(8,128)(2,1)}, bf16[64,512]{1,0:T(8,128)(2,1)}) custom-call(bf16[2,224,2048]{2,1,0:T(8,128)(2,1)} %get-tuple-element.12.refs_0_, bf16[2,224,2048]{2,1,0:T(8,128)(2,1)} %get-tuple-element.13.refs_1_, ...), custom_call_target="tpu_custom_call" | custom-call | tf_op jit(solution)/shard_map/deliver/pallas_call | solution.py:493

commit v6 on v5

--- a/solution.py
+++ b/solution.py
@@ -13,6 +13,7 @@
 FS = ("z", "y", "c")
 HOPS = (1, 3, 2)
 STEPS = HOPS + (0,)
+FARTHEST_FIRST = (2, 0, 1, 3)
 ROWS = ((0, 96), (96, 80), (176, 80))
 ROUTES = ((0, 64, "xyz"), (64, 96, "xzy"), (160, 96, "zyx"))
 CHUNKS = 12
@@ -41,10 +42,10 @@
 def whole(gate, up, down, gain, hidden, ids, logits,
           gate_out, up_out, down_out, out,
           raw, doubled, gains, sent, over_x, over_z, served, tokens, chip, shares, near_shares, share_cols,
-          wide, acts, give, near, held, one0, one1, one2, add0, add1, add2,
+          wide, acts, give, near, held, one0, one1, one2, carry0, carry1, carry2, add0, add1, add2,
           two0, two1, two2, sum0, sum1, sum2, three0, three1, three2, last, turned,
           ls, ps, pr, credit, xs, xr, zs, zr, ys, yr, hs, hr, ns, nr, ws, wr,
-          gs, gr, hops, hopr, cs, cr, os, ds, dr, fs, fr, ss, sr, ts, tr, es, er):
+          gs, gr, hops, hopr, cs, cr, os, ds, dr, ks, kr0, kr, fs, fr, ss, sr, ts, tr, es, er):
     masters = (gate, up, down)
     outs = (gate_out, up_out, down_out)
     x, y, z, c = (lax.axis_index(a) for a in ("x", "y", "z", "c"))
@@ -310,9 +311,9 @@
     act_block(0)
     y_step(10)
     pass_on(2)
-    y_step(11)
     arrived(flows["c", 4])
     act_block(1)
+    y_step(11)
     arrived(flows["p", 2])
     to_core(5, part(2, 2, {"x": along("x", 2)}))
     arrived(flows["c", 3])
@@ -329,30 +330,80 @@
         v = jnp.dot(acts[0, rows], served[2, 0, :, cols], preferred_element_type=jnp.float32)
         return v + jnp.dot(acts[1, rows], served[2, 1, :, cols], preferred_element_type=jnp.float32)
 
-    given = []
-    for i, h in enumerate(STEPS):
-        t = along("x", h) * 2 + 1 - c
+    given = {}
+    for i in FARTHEST_FIRST:
+        t = along("x", STEPS[i]) * 2 + 1 - c
         for n in range(4):
             v = down_part(t, n)
             for b in range(4):
                 give[i, n, b] = v[:, 128 * b : 128 * b + 128].astype(jnp.bfloat16)
-        given.append(start(push(give.at[i], near.at[i], ds.at[i], dr.at[i], other)))
+        given[i] = [start(push(give.at[i], near.at[i], ds.at[i], dr.at[i], other))]
     r0, r1, r2 = (pl.ds(*r) for r in ROWS)
     every = slice(None)
-    for i, h in enumerate(STEPS):
-        t = along("x", h) * 2 + c
-        arrived([given[i]])
+    quarter = ROWS[0][1] // 2
+    low, high = pl.ds(0, quarter), pl.ds(quarter, quarter)
+
+    def y_block(zz, hop, i):
+        return held.at[zz, along("y", hop), i, r1]
+
+    def z_block(yy, hop, i):
+        return held.at[along("z", hop), yy, i, r2]
+
+    routes = ((1, "y", y_block, one1, carry1), (2, "z", z_block, one2, carry2))
+    pairs = (slice(0, 2), slice(2, 4))
+
+    def send_first(i):
+        if i == 2:
+            for d, h in enumerate((1, 3)):
+                block = held.at[every, every, 2, (low, high)[d]]
+                push(block, carry0.at[d], ks.at[0], kr0.at[d], {"x": along("x", h)}).start()
+        if i < 2:
+            h, rows = STEPS[i], (high, low)[i]
+            push(held.at[every, every, i, rows], one0.at[i, every, every, rows], fs.at[0], fr.at[0],
+                 {"x": along("x", h)}).start()
+        for l, axis, block, one, carry in routes:
+            for d, h in enumerate((1, 3)):
+                peer = {axis: along(axis, h)}
+                push(block(pairs[d], 2, i), carry.at[d, i], ks.at[l], kr.at[l - 1, d, i], peer).start()
+            for d, h in enumerate((1, 3)):
+                peer = {axis: along(axis, h)}
+                rest = pairs[1 - d]
+                push(block(rest, h, i), one.at[d, rest, i], fs.at[l], fr.at[l], peer).start()
+
+    def send_carried(i):
+        if i == 2:
+            for d, h in enumerate((1, 3)):
+                bulk(carry0.at[d], ks.at[0], kr0.at[d]).wait_recv()
+                rows = (low, high)[d]
+
+                def body(n, carry):
+                    a, b = n // 4, lax.rem(n, 4)
+                    v = held[a, b, d, rows].astype(jnp.float32) + carry0[d, a, b].astype(jnp.float32)
+                    held[a, b, d, rows] = v.astype(jnp.bfloat16)
+                    return carry
+
+                lax.fori_loop(0, 16, body, 0)
+                push(held.at[every, every, d, rows], one0.at[d, every, every, rows], fs.at[0], fr.at[0],
+                     {"x": along("x", h)}).start()
+        for l, axis, block, one, carry in routes:
+            for d, h in enumerate((1, 3)):
+                bulk(carry.at[d, i], ks.at[l], kr.at[l - 1, d, i]).wait_recv()
+                ref = block(pairs[d], h, i)
+                ref[...] = (ref[...].astype(jnp.float32) + carry[d, i].astype(jnp.float32)).astype(jnp.bfloat16)
+                push(block(pairs[d], h, i), one.at[d, pairs[d], i], fs.at[l], fr.at[l],
+                     {axis: along(axis, h)}).start()
+
+    for i in FARTHEST_FIRST:
+        t = along("x", STEPS[i]) * 2 + c
+        arrived(given[i])
         for n in range(4):
             v = down_part(t, n)
             for b in range(4):
                 total = v[:, 128 * b : 128 * b + 128] + near[i, n, b].astype(jnp.float32)
                 held[n, b, i] = total.astype(jnp.bfloat16)
-        if i < 3:
-            push(held.at[every, every, i, r0], one0.at[i], fs.at[0], fr.at[0], {"x": along("x", h)}).start()
-        for j, g in enumerate(HOPS):
-            py, pz = along("y", g), along("z", g)
-            push(held.at[every, py, i, r1], one1.at[j, :, i], fs.at[1], fr.at[1], {"y": py}).start()
-            push(held.at[pz, every, i, r2], one2.at[j, :, i], fs.at[2], fr.at[2], {"z": pz}).start()
+        send_first(i)
+    for i in FARTHEST_FIRST:
+        send_carried(i)
 
     def summed(base, terms):
         v = base.astype(jnp.float32)
@@ -369,7 +420,7 @@
 
         def body(n, carry):
             a, b = n // 4, lax.rem(n, 4)
-            adds[l][a, b] = summed(base(a, b), [ones[l][j, a, b] for j in range(3)]).astype(jnp.bfloat16)
+            adds[l][a, b] = summed(base(a, b), [ones[l][j, a, b] for j in range(2)]).astype(jnp.bfloat16)
             return carry
 
         lax.fori_loop(0, 16, body, 0)
@@ -410,6 +461,8 @@
     bulk(over_z.at[:, 0:3], zs, zr.at[0]).wait_send()
     for rc in range(2):
         bulk(over_z.at[0:6, 0 : 3 + rc], ys.at[rc], yr.at[0]).wait_send()
+    for l, carry in enumerate((carry0, carry1, carry2)):
+        bulk(carry, ks.at[l], fr.at[l]).wait_send()
     for l in range(3):
         bulk(ones[l], fs.at[l], fr.at[l]).wait_send()
         bulk(twos[l], ss.at[l], sr.at[l]).wait_send()
@@ -442,7 +495,8 @@
         + [pltpu.VMEM((4, 8, 512), f32)] * 2
         + [pltpu.VMEM((2048, 128), f32)]
         + buffers((256, 2048), (2, 2048, 224), (4, 4, 4, 256, 128), (4, 4, 4, 256, 128), (4, 4, 4, 256, 128))
-        + buffers(*[(3, 4, 4, n, 128) for n in sizes])
+        + buffers(*[(2, 4, 4, n, 128) for n in sizes])
+        + buffers((2, 4, 4, sizes[0] // 2, 128), (2, 4, 2, sizes[1], 128), (2, 4, 2, sizes[2], 128))
         + buffers(*[(4, 4, n, 128) for n in sizes])
         + buffers(*[(3, 4, n, 128) for n in sizes])
         + buffers(*[(4, n, 128) for n in sizes])
@@ -457,6 +511,7 @@
         + [dma((6,))] * 2
         + [dma((3,))]
         + [dma((4,))] * 2
+        + [dma((3,)), dma((2,)), dma((2, 2, 4))]
         + [dma((3,))] * 6
         + [dma] * 2,
         compiler_params=pltpu.CompilerParams(

time: 144 us -> 139 us (0.965)
  Pallas kernels: 143 us -> 138 us
    pallas_call x1, Pallas kernels: 138 us -> 133 us  [whole_call(): pl.pallas_call(whole, out_shape=(served, served, served, jax.ShapeDtypeSt...]
where the time goes in v6:
time: 139 us
  Pallas kernels  138 us (99%)
    pallas_call x1, Pallas kernels, whole_call(): pl.pallas_call(whole, out_shape=(served, served, served, jax.ShapeDtypeSt...  133 us
    pallas_call x1, Pallas kernels, deliver_call(): pl.pallas_call(deliver, out_shape=tuple((jax.ShapeDtypeStruct(r.shape, r....  5.05 us

profile of v6, /device:TPU:1, one launch (start us, length us, event | category | flops | bytes accessed | tf_op | source)
XLA Modules:
  0.0 138.8 jit_solution(14471022779160036818)
XLA Ops:
  0.6 133.1 %whole.1 = (bf16[2,224,2048]{2,1,0:T(8,128)(2,1)}, bf16[2,224,2048]{2,1,0:T(8,128)(2,1)}, bf16[2,224,2048]{2,1,0:T(8,128)(2,1)}, bf16[64,512]{1,0:T(8,128)(2,1)}) custom-call(f32[4,2,64,1792]{3,2,1,0:T(8,128)} %bitcast.11, f32[4,2,64,1792]{3,2,1,0:T(8,128)} %bitcast.12, f32[4,2,64,1792]{3,2,1,0:T(8,128)} %bitcast.13, f32[1,64]{1,0:T(1,128)} %bitcast.17, ...), custom_call_target="tpu_custom_call" | custom-call | tf_op jit(solution)/shard_map/whole/pallas_call | solution.py:487
  133.8 5.1 %deliver.1 = (bf16[2,224,2048]{2,1,0:T(8,128)(2,1)}, bf16[2,224,2048]{2,1,0:T(8,128)(2,1)}, bf16[2,224,2048]{2,1,0:T(8,128)(2,1)}, bf16[64,512]{1,0:T(8,128)(2,1)}) custom-call(bf16[2,224,2048]{2,1,0:T(8,128)(2,1)} %get-tuple-element.12.refs_0_, bf16[2,224,2048]{2,1,0:T(8,128)(2,1)} %get-tuple-element.13.refs_1_, ...), custom_call_target="tpu_custom_call" | custom-call | tf_op jit(solution)/shard_map/deliver/pallas_call | solution.py:548

commit v7 on v6

--- a/solution.py
+++ b/solution.py
@@ -17,6 +17,7 @@
 ROWS = ((0, 96), (96, 80), (176, 80))
 ROUTES = ((0, 64, "xyz"), (64, 96, "xzy"), (160, 96, "zyx"))
 CHUNKS = 12
+PARTS = tuple((k, 0, 112) for k in range(4)) + tuple((k, r, n) for k in range(4, CHUNKS) for r, n in ((0, 64), (64, 48)))
 
 
 def along(axis, hop):
@@ -181,49 +182,56 @@
     def split(k):
         return k // 4, (k // 2) % 2, k % 2
 
-    def x_send(k, i):
+    def x_send(p, i):
+        k, r, n = PARTS[p]
         m, hh, rc = split(k)
         peer = along("x", HOPS[i])
-        src = sent.at[m, peer, :, lax.rem(c + rc, 2), hh]
-        push(src, over_x.at[k, x], xs, xr.at[k], {"x": peer}).start()
+        src = sent.at[m, peer, :, lax.rem(c + rc, 2), hh, pl.ds(r, n)]
+        push(src, over_x.at[k, x, :, pl.ds(r, n)], xs, xr.at[p], {"x": peer}).start()
 
     def x_keep(k):
         m, hh, rc = split(k)
         over_x[k, x] = sent[m, x, :, lax.rem(c + rc, 2), hh]
 
     def x_steps(m):
-        for k in range(4 * m, 4 * m + 4):
-            for i in range(3):
-                x_send(k, i)
+        for p, (k, _, _) in enumerate(PARTS):
+            if k // 4 == m:
+                for i in range(3):
+                    x_send(p, i)
         for k in range(4 * m, 4 * m + 4):
             x_keep(k)
 
-    def z_step(k):
-        bulk(over_x.at[k, 0:3], xs, xr.at[k]).wait_recv()
+    def z_step(p):
+        k, r, n = PARTS[p]
+        rows = pl.ds(r, n)
+        bulk(over_x.at[k, 0:3, :, rows], xs, xr.at[p]).wait_recv()
         for h in HOPS:
             peer = along("z", h)
-            push(over_x.at[k, peer], over_z.at[k, z], zs, zr.at[k], {"z": peer}).start()
-        over_z[k, z] = over_x[k, z]
+            push(over_x.at[k, peer, :, rows], over_z.at[k, z, :, rows], zs, zr.at[p], {"z": peer}).start()
+        over_z[k, z, :, rows] = over_x[k, z, :, rows]
 
     def lanes(zz):
         return pl.ds(pl.multiple_of((zz * 4 + y) * 128, 128), 128)
 
-    def y_step(k):
+    def y_step(p):
+        k, r, n = PARTS[p]
         m, hh, rc = split(k)
-        bulk(over_z.at[k, 0:3], zs, zr.at[k]).wait_recv()
-        rows = pl.ds(hh * 112, 112)
+        bulk(over_z.at[k, 0:3, :, pl.ds(r, n)], zs, zr.at[p]).wait_recv()
+        rows = pl.ds(hh * 112 + r, n)
         for h in STEPS if rc else HOPS:
             py = along("y", h)
             peer = {"y": py, "c": lax.rem(c + rc, 2)}
             for zz in range(4):
-                push(over_z.at[k, zz, py], served.at[m, c, rows, lanes(zz)], ys.at[rc], yr.at[k], peer).start()
+                push(over_z.at[k, zz, py, pl.ds(r, n)], served.at[m, c, rows, lanes(zz)],
+                     ys.at[rc], yr.at[p], peer).start()
         if rc == 0:
             for zz in range(4):
-                served[m, c, rows, lanes(zz)] = over_z[k, zz, y]
-
-    def y_landed(k):
+                served[m, c, rows, lanes(zz)] = over_z[k, zz, y, pl.ds(r, n)]
+
+    def y_landed(p):
+        k, r, n = PARTS[p]
         rc = k % 2
-        bulk(over_z.at[k, 0 : 3 + rc], ys.at[rc], yr.at[k]).wait_recv()
+        bulk(over_z.at[k, 0 : 3 + rc, :, pl.ds(r, n)], ys.at[rc], yr.at[p]).wait_recv()
 
     for i, h in enumerate(STEPS):
         loaded(0, i)
@@ -265,63 +273,77 @@
         cp.start()
         stores.append(cp)
 
-    def act_tile(xb, ch):
-        t = xb * 2 + ch
-        total = jnp.zeros((256, 128), jnp.float32)
+    early, late = ROUTES[2][0], ROUTES[2][1]
+
+    def act_rows(blocks, first, count):
+        m = count * len(blocks)
+        total = jnp.zeros((m, 128), jnp.float32)
         for q in range(16):
-            block = tokens[q // 4, q % 4, xb, ch]
-            wide[:, 128 * q : 128 * q + 128] = block
+            block = [tokens[q // 4, q % 4, xb, ch, first : first + count] for xb, ch in blocks]
+            block = jnp.concatenate(block, axis=0)
+            wide[0:m, 128 * q : 128 * q + 128] = block
             v = block.astype(jnp.float32)
             total = total + v * v
         inv = lax.rsqrt(jnp.sum(total, axis=1, keepdims=True) / 2048.0 + EPSILON)
         dims = (((1,), (1,)), ((), ()))
-        rows = pl.ds(pl.multiple_of(t * 256, 256), 256)
         for e in range(2):
-            gate_pre = lax.dot_general(wide[...], served[0, e], dims, preferred_element_type=jnp.float32) * inv
-            up_pre = lax.dot_general(wide[...], served[1, e], dims, preferred_element_type=jnp.float32) * inv
+            gate_pre = lax.dot_general(wide[0:m], served[0, e], dims, preferred_element_type=jnp.float32) * inv
+            up_pre = lax.dot_general(wide[0:m], served[1, e], dims, preferred_element_type=jnp.float32) * inv
             act = gate_pre / (1.0 + jnp.exp(-gate_pre)) * up_pre
-            acts[e, rows] = (act * share_cols[rows, e : e + 1]).astype(jnp.bfloat16)
-
-    def act_block(hop):
-        def one(ch, carry):
-            act_tile(along("x", hop), ch)
-            return carry
-
-        lax.fori_loop(0, 2, one, 0)
-
-    for k in range(9):
-        if k < 8:
-            z_step(k + 2)
-        if k == 1:
+            for n, (xb, ch) in enumerate(blocks):
+                rows = pl.ds(pl.multiple_of((xb * 2 + ch) * 256 + first, 16), count)
+                piece = act[count * n : count * n + count] * share_cols[rows, e : e + 1]
+                acts[e, rows] = piece.astype(jnp.bfloat16)
+
+    def act_early(xb):
+        act_rows([(xb, 0), (xb, 1)], 0, early)
+
+    def act_late(hops):
+        act_rows([(along("x", h), ch) for h in hops for ch in (0, 1)], early, late)
+
+    ahead = 2
+    for p in range(14):
+        while ahead <= min(p + (2 if p < 4 else 4), 19):
+            z_step(ahead)
+            ahead += 1
+        if p == 1:
             pass_on(0)
             pass_on(1)
-        if k in (5, 6):
-            arrived(flows["p", k - 5])
-            to_core(k - 5, part(k - 5, 3))
-        y_step(k)
-    z_step(10)
-    z_step(11)
-    y_step(9)
-    for k in range(8):
-        y_landed(k)
+        if p in (6, 8):
+            n = (p - 6) // 2
+            arrived(flows["p", n])
+            to_core(n, part(n, 3))
+        y_step(p)
+    z_step(18)
+    z_step(19)
+    for p in range(12):
+        y_landed(p)
     store(0)
     store(1)
-    for n in range(3):
+    for n in range(2):
         arrived(flows["c", n])
-    act_block(0)
-    y_step(10)
+    act_early(0)
+    y_step(14)
+    act_early(1)
+    y_step(15)
+    act_early(2)
+    y_step(16)
+    act_early(3)
+    y_step(17)
     pass_on(2)
+    arrived(flows["c", 2])
+    act_late((0,))
+    y_step(18)
     arrived(flows["c", 4])
-    act_block(1)
-    y_step(11)
+    arrived(flows["c", 3])
+    act_late((1, 3))
+    y_step(19)
     arrived(flows["p", 2])
     to_core(5, part(2, 2, {"x": along("x", 2)}))
-    arrived(flows["c", 3])
-    act_block(3)
     arrived(flows["c", 5])
-    act_block(2)
-    for k in range(8, 12):
-        y_landed(k)
+    act_late((2,))
+    for p in range(12, 20):
+        y_landed(p)
     store(2)
 
     def down_part(t, n):
@@ -494,7 +516,7 @@
                   (3, 2, 224, 2048), (4, 4, 4, 2, 256, 128), (128, 256))
         + [pltpu.VMEM((4, 8, 512), f32)] * 2
         + [pltpu.VMEM((2048, 128), f32)]
-        + buffers((256, 2048), (2, 2048, 224), (4, 4, 4, 256, 128), (4, 4, 4, 256, 128), (4, 4, 4, 256, 128))
+        + buffers((384, 2048), (2, 2048, 224), (4, 4, 4, 256, 128), (4, 4, 4, 256, 128), (4, 4, 4, 256, 128))
         + buffers(*[(2, 4, 4, n, 128) for n in sizes])
         + buffers((2, 4, 4, sizes[0] // 2, 128), (2, 4, 2, sizes[1], 128), (2, 4, 2, sizes[2], 128))
         + buffers(*[(4, 4, n, 128) for n in sizes])
@@ -503,7 +525,7 @@
         + buffers(*[(3, n, 128) for n in sizes])
         + buffers((256, 128), (128, 256))
         + [dma((6,)), dma, dma((6,)), pltpu.SemaphoreType.REGULAR]
-        + [dma, dma((CHUNKS,)), dma, dma((CHUNKS,)), dma((2,)), dma((CHUNKS,))]
+        + [dma, dma((len(PARTS),)), dma, dma((len(PARTS),)), dma((2,)), dma((len(PARTS),))]
         + [dma] * 4
         + [dma((3,))] * 2
         + [dma((3, 2, 3))] * 2

time: 139 us -> 135 us (0.971)
  Pallas kernels: 138 us -> 134 us
    pallas_call x1, Pallas kernels: 133 us -> 129 us  [whole_call(): pl.pallas_call(whole, out_shape=(served, served, served, jax.ShapeDtypeSt...]
where the time goes in v7:
time: 135 us
  Pallas kernels  134 us (99%)
    pallas_call x1, Pallas kernels, whole_call(): pl.pallas_call(whole, out_shape=(served, served, served, jax.ShapeDtypeSt...  129 us
    pallas_call x1, Pallas kernels, deliver_call(): pl.pallas_call(deliver, out_shape=tuple((jax.ShapeDtypeStruct(r.shape, r....  5.05 us

profile of v7, /device:TPU:1, one launch (start us, length us, event | category | flops | bytes accessed | tf_op | source)
XLA Modules:
  0.0 135.1 jit_solution(1661213967076818035)
XLA Ops:
  0.6 129.2 %whole.1 = (bf16[2,224,2048]{2,1,0:T(8,128)(2,1)}, bf16[2,224,2048]{2,1,0:T(8,128)(2,1)}, bf16[2,224,2048]{2,1,0:T(8,128)(2,1)}, bf16[64,512]{1,0:T(8,128)(2,1)}) custom-call(f32[4,2,64,1792]{3,2,1,0:T(8,128)} %bitcast.11, f32[4,2,64,1792]{3,2,1,0:T(8,128)} %bitcast.12, f32[4,2,64,1792]{3,2,1,0:T(8,128)} %bitcast.13, f32[1,64]{1,0:T(1,128)} %bitcast.17, ...), custom_call_target="tpu_custom_call" | custom-call | tf_op jit(solution)/shard_map/whole/pallas_call | solution.py:509
  129.8 5.1 %deliver.1 = (bf16[2,224,2048]{2,1,0:T(8,128)(2,1)}, bf16[2,224,2048]{2,1,0:T(8,128)(2,1)}, bf16[2,224,2048]{2,1,0:T(8,128)(2,1)}, bf16[64,512]{1,0:T(8,128)(2,1)}) custom-call(bf16[2,224,2048]{2,1,0:T(8,128)(2,1)} %get-tuple-element.12.refs_0_, bf16[2,224,2048]{2,1,0:T(8,128)(2,1)} %get-tuple-element.13.refs_1_, ...), custom_call_target="tpu_custom_call" | custom-call | tf_op jit(solution)/shard_map/deliver/pallas_call | solution.py:570

commit v8 on v7

--- a/solution.py
+++ b/solution.py
@@ -17,7 +17,7 @@
 ROWS = ((0, 96), (96, 80), (176, 80))
 ROUTES = ((0, 64, "xyz"), (64, 96, "xzy"), (160, 96, "zyx"))
 CHUNKS = 12
-PARTS = tuple((k, 0, 112) for k in range(4)) + tuple((k, r, n) for k in range(4, CHUNKS) for r, n in ((0, 64), (64, 48)))
+PARTS = tuple((k, r, n) for k in range(CHUNKS) for r, n in ((0, 64), (64, 48)))
 
 
 def along(axis, hop):
@@ -43,10 +43,10 @@
 def whole(gate, up, down, gain, hidden, ids, logits,
           gate_out, up_out, down_out, out,
           raw, doubled, gains, sent, over_x, over_z, served, tokens, chip, shares, near_shares, share_cols,
-          wide, acts, give, near, held, one0, one1, one2, carry0, carry1, carry2, add0, add1, add2,
+          wide, acts, far_acts, far_down, held, one0, one1, one2, carry0, carry1, carry2, add0, add1, add2,
           two0, two1, two2, sum0, sum1, sum2, three0, three1, three2, last, turned,
           ls, ps, pr, credit, xs, xr, zs, zr, ys, yr, hs, hr, ns, nr, ws, wr,
-          gs, gr, hops, hopr, cs, cr, os, ds, dr, ks, kr0, kr, fs, fr, ss, sr, ts, tr, es, er):
+          gs, gr, hops, hopr, cs, cr, os, das, dar, dws, dwr, ks, kr0, kr, fs, fr, ss, sr, ts, tr, es, er):
     masters = (gate, up, down)
     outs = (gate_out, up_out, down_out)
     x, y, z, c = (lax.axis_index(a) for a in ("x", "y", "z", "c"))
@@ -238,9 +238,9 @@
         pack_one(0, along("x", h))
         if i < 3:
             x_send(0, i)
-    for k in range(1, 4):
+    for p in range(1, 8):
         for i in range(3):
-            x_send(k, i)
+            x_send(p, i)
     for l in range(3):
         arrived(flows["g", l, 0])
         gather(l, 1)
@@ -249,6 +249,7 @@
     for k in range(4):
         x_keep(k)
     z_step(0)
+    z_step(1)
     for l in range(2):
         arrived(flows["g", l, 1])
         spread_out(l)
@@ -258,7 +259,8 @@
     x_steps(1)
     arrived(flows["g", 2, 1])
     to_core(2, part(2, 2))
-    z_step(1)
+    z_step(2)
+    z_step(3)
     pack(2)
     x_steps(2)
     spread_out(2)
@@ -295,71 +297,92 @@
                 piece = act[count * n : count * n + count] * share_cols[rows, e : e + 1]
                 acts[e, rows] = piece.astype(jnp.bfloat16)
 
+    def swap_acts(i):
+        rows = pl.ds(pl.multiple_of((along("x", STEPS[i]) * 2 + 1 - c) * 256, 256), 256)
+        for e in range(2):
+            push(acts.at[e, rows], far_acts.at[i, e], das, dar.at[i], other).start()
+
+    def swap_down(p):
+        k, r, n = PARTS[p]
+        _, hh, rc = split(k)
+        y_landed(p)
+        rows = pl.ds(hh * 112 + r, n)
+        e = lax.rem(c + rc, 2)
+        push(served.at[2, e, rows], far_down.at[e, rows], dws, dwr.at[p - 16], other).start()
+
     def act_early(xb):
         act_rows([(xb, 0), (xb, 1)], 0, early)
 
     def act_late(hops):
         act_rows([(along("x", h), ch) for h in hops for ch in (0, 1)], early, late)
 
-    ahead = 2
-    for p in range(14):
-        while ahead <= min(p + (2 if p < 4 else 4), 19):
+    ahead = 4
+    for p in range(18):
+        while ahead <= p + (3 if p < 8 else 4):
             z_step(ahead)
             ahead += 1
-        if p == 1:
+        if p == 3:
             pass_on(0)
             pass_on(1)
-        if p in (6, 8):
-            n = (p - 6) // 2
+        if p in (10, 12):
+            n = (p - 10) // 2
             arrived(flows["p", n])
             to_core(n, part(n, 3))
         y_step(p)
-    z_step(18)
-    z_step(19)
-    for p in range(12):
+    z_step(22)
+    z_step(23)
+    for p in range(16):
         y_landed(p)
     store(0)
     store(1)
     for n in range(2):
         arrived(flows["c", n])
     act_early(0)
-    y_step(14)
+    y_step(18)
     act_early(1)
-    y_step(15)
+    y_step(19)
     act_early(2)
-    y_step(16)
+    y_step(20)
     act_early(3)
-    y_step(17)
+    y_step(21)
     pass_on(2)
     arrived(flows["c", 2])
     act_late((0,))
-    y_step(18)
+    y_step(22)
+    swap_acts(3)
+    for p in range(16, 20):
+        swap_down(p)
     arrived(flows["c", 4])
     arrived(flows["c", 3])
     act_late((1, 3))
-    y_step(19)
+    y_step(23)
+    swap_acts(0)
+    swap_acts(1)
+    swap_down(20)
+    swap_down(21)
     arrived(flows["p", 2])
     to_core(5, part(2, 2, {"x": along("x", 2)}))
     arrived(flows["c", 5])
     act_late((2,))
-    for p in range(12, 20):
-        y_landed(p)
+    swap_acts(2)
+    swap_down(22)
+    swap_down(23)
     store(2)
 
-    def down_part(t, n):
-        rows = pl.ds(pl.multiple_of(t * 256, 256), 256)
+    def down_part(i, n):
+        rows = pl.ds(pl.multiple_of((along("x", STEPS[i]) * 2 + c) * 256, 256), 256)
         cols = slice(512 * n, 512 * n + 512)
-        v = jnp.dot(acts[0, rows], served[2, 0, :, cols], preferred_element_type=jnp.float32)
-        return v + jnp.dot(acts[1, rows], served[2, 1, :, cols], preferred_element_type=jnp.float32)
-
-    given = {}
-    for i in FARTHEST_FIRST:
-        t = along("x", STEPS[i]) * 2 + 1 - c
-        for n in range(4):
-            v = down_part(t, n)
-            for b in range(4):
-                give[i, n, b] = v[:, 128 * b : 128 * b + 128].astype(jnp.bfloat16)
-        given[i] = [start(push(give.at[i], near.at[i], ds.at[i], dr.at[i], other))]
+        v = 0.0
+        for e in range(2):
+            v = v + jnp.dot(acts[e, rows], served[2, e, :, cols], preferred_element_type=jnp.float32)
+        for e in range(2):
+            v = v + jnp.dot(far_acts[i, e], far_down[e, :, cols], preferred_element_type=jnp.float32)
+        return v
+
+    for p in range(16, 24):
+        k, r, n = PARTS[p]
+        block = far_down.at[0, pl.ds(0, n)]
+        bulk(block, dws, dwr.at[p - 16]).wait_recv()
     r0, r1, r2 = (pl.ds(*r) for r in ROWS)
     every = slice(None)
     quarter = ROWS[0][1] // 2
@@ -416,13 +439,11 @@
                      {axis: along(axis, h)}).start()
 
     for i in FARTHEST_FIRST:
-        t = along("x", STEPS[i]) * 2 + c
-        arrived(given[i])
+        bulk(far_acts.at[i], das, dar.at[i]).wait_recv()
         for n in range(4):
-            v = down_part(t, n)
+            v = down_part(i, n).astype(jnp.bfloat16)
             for b in range(4):
-                total = v[:, 128 * b : 128 * b + 128] + near[i, n, b].astype(jnp.float32)
-                held[n, b, i] = total.astype(jnp.bfloat16)
+                held[n, b, i] = v[:, 128 * b : 128 * b + 128]
         send_first(i)
     for i in FARTHEST_FIRST:
         send_carried(i)
@@ -454,8 +475,8 @@
 
     def send_on(l, s, pick, dst, send, recv):
         axis = turns[l][s]
-        for j, h in enumerate(HOPS):
-            peer = along(axis, h)
+        for j in (2, 0, 1):
+            peer = along(axis, HOPS[j])
             push(pick(j, peer), dst.at[j], send.at[l], recv.at[l], {axis: peer}).start()
 
     bases = (lambda a, b: held[a, b, 3, r0], lambda a, b: held[a, y, b, r1], lambda a, b: held[z, a, b, r2])
@@ -483,6 +504,8 @@
     bulk(over_z.at[:, 0:3], zs, zr.at[0]).wait_send()
     for rc in range(2):
         bulk(over_z.at[0:6, 0 : 3 + rc], ys.at[rc], yr.at[0]).wait_send()
+    bulk(far_acts, das, dar.at[0]).wait_send()
+    bulk(far_down, dws, dwr.at[0]).wait_send()
     for l, carry in enumerate((carry0, carry1, carry2)):
         bulk(carry, ks.at[l], fr.at[l]).wait_send()
     for l in range(3):
@@ -516,7 +539,7 @@
                   (3, 2, 224, 2048), (4, 4, 4, 2, 256, 128), (128, 256))
         + [pltpu.VMEM((4, 8, 512), f32)] * 2
         + [pltpu.VMEM((2048, 128), f32)]
-        + buffers((384, 2048), (2, 2048, 224), (4, 4, 4, 256, 128), (4, 4, 4, 256, 128), (4, 4, 4, 256, 128))
+        + buffers((384, 2048), (2, 2048, 224), (4, 2, 256, 224), (2, 224, 2048), (4, 4, 4, 256, 128))
         + buffers(*[(2, 4, 4, n, 128) for n in sizes])
         + buffers((2, 4, 4, sizes[0] // 2, 128), (2, 4, 2, sizes[1], 128), (2, 4, 2, sizes[2], 128))
         + buffers(*[(4, 4, n, 128) for n in sizes])
@@ -532,7 +555,7 @@
         + [dma((3, 4))] * 2
         + [dma((6,))] * 2
         + [dma((3,))]
-        + [dma((4,))] * 2
+        + [dma, dma((4,)), dma, dma((8,))]
         + [dma((3,)), dma((2,)), dma((2, 2, 4))]
         + [dma((3,))] * 6
         + [dma] * 2,

time: 135 us -> 134 us (level)
    pallas_call x1, Pallas kernels: 129 us -> 128 us  [whole_call(): pl.pallas_call(whole, out_shape=(served, served, served, jax.ShapeDtypeSt...]
where the time goes in v8:
time: 134 us
  Pallas kernels  133 us (99%)
    pallas_call x1, Pallas kernels, whole_call(): pl.pallas_call(whole, out_shape=(served, served, served, jax.ShapeDtypeSt...  128 us
    pallas_call x1, Pallas kernels, deliver_call(): pl.pallas_call(deliver, out_shape=tuple((jax.ShapeDtypeStruct(r.shape, r....  5.05 us

profile of v8, /device:TPU:1, one launch (start us, length us, event | category | flops | bytes accessed | tf_op | source)
XLA Modules:
  0.0 133.6 jit_solution(13161137275600215394)
XLA Ops:
  0.6 127.8 %whole.1 = (bf16[2,224,2048]{2,1,0:T(8,128)(2,1)}, bf16[2,224,2048]{2,1,0:T(8,128)(2,1)}, bf16[2,224,2048]{2,1,0:T(8,128)(2,1)}, bf16[64,512]{1,0:T(8,128)(2,1)}) custom-call(f32[4,2,64,1792]{3,2,1,0:T(8,128)} %bitcast.11, f32[4,2,64,1792]{3,2,1,0:T(8,128)} %bitcast.12, f32[4,2,64,1792]{3,2,1,0:T(8,128)} %bitcast.13, f32[1,64]{1,0:T(1,128)} %bitcast.17, ...), custom_call_target="tpu_custom_call" | custom-call | tf_op jit(solution)/shard_map/whole/pallas_call | solution.py:532
  128.4 5.1 %deliver.1 = (bf16[2,224,2048]{2,1,0:T(8,128)(2,1)}, bf16[2,224,2048]{2,1,0:T(8,128)(2,1)}, bf16[2,224,2048]{2,1,0:T(8,128)(2,1)}, bf16[64,512]{1,0:T(8,128)(2,1)}) custom-call(bf16[2,224,2048]{2,1,0:T(8,128)(2,1)} %get-tuple-element.12.refs_0_, bf16[2,224,2048]{2,1,0:T(8,128)(2,1)} %get-tuple-element.13.refs_1_, ...), custom_call_target="tpu_custom_call" | custom-call | tf_op jit(solution)/shard_map/deliver/pallas_call | solution.py:593

commit v9 on v8

--- a/solution.py
+++ b/solution.py
@@ -369,16 +369,21 @@
     swap_down(23)
     store(2)
 
-    def down_part(i, n):
+    def down_near(i, n):
         rows = pl.ds(pl.multiple_of((along("x", STEPS[i]) * 2 + c) * 256, 256), 256)
         cols = slice(512 * n, 512 * n + 512)
         v = 0.0
         for e in range(2):
             v = v + jnp.dot(acts[e, rows], served[2, e, :, cols], preferred_element_type=jnp.float32)
+        return v
+
+    def down_far(i, n, v):
+        cols = slice(512 * n, 512 * n + 512)
         for e in range(2):
             v = v + jnp.dot(far_acts[i, e], far_down[e, :, cols], preferred_element_type=jnp.float32)
         return v
 
+    nears = [down_near(FARTHEST_FIRST[0], n) for n in range(4)]
     for p in range(16, 24):
         k, r, n = PARTS[p]
         block = far_down.at[0, pl.ds(0, n)]
@@ -398,10 +403,6 @@
     pairs = (slice(0, 2), slice(2, 4))
 
     def send_first(i):
-        if i == 2:
-            for d, h in enumerate((1, 3)):
-                block = held.at[every, every, 2, (low, high)[d]]
-                push(block, carry0.at[d], ks.at[0], kr0.at[d], {"x": along("x", h)}).start()
         if i < 2:
             h, rows = STEPS[i], (high, low)[i]
             push(held.at[every, every, i, rows], one0.at[i, every, every, rows], fs.at[0], fr.at[0],
@@ -441,9 +442,14 @@
     for i in FARTHEST_FIRST:
         bulk(far_acts.at[i], das, dar.at[i]).wait_recv()
         for n in range(4):
-            v = down_part(i, n).astype(jnp.bfloat16)
+            v = nears[n] if i == FARTHEST_FIRST[0] else down_near(i, n)
+            v = down_far(i, n, v).astype(jnp.bfloat16)
             for b in range(4):
                 held[n, b, i] = v[:, 128 * b : 128 * b + 128]
+            if i == 2:
+                for d, h in enumerate((1, 3)):
+                    block = held.at[n, every, 2, (low, high)[d]]
+                    push(block, carry0.at[d, n], ks.at[0], kr0.at[d], {"x": along("x", h)}).start()
         send_first(i)
     for i in FARTHEST_FIRST:
         send_carried(i)

time: 134 us -> 133 us (level)
  no operation moved by 1% of the time
where the time goes in v9:
time: 133 us; the launch traced here: 132 us
  Pallas kernels  132 us (99%)
    pallas_call x1, Pallas kernels, whole_call(): pl.pallas_call(whole, out_shape=(served, served, served, jax.ShapeDtypeSt...  127 us
    pallas_call x1, Pallas kernels, deliver_call(): pl.pallas_call(deliver, out_shape=tuple((jax.ShapeDtypeStruct(r.shape, r....  5.05 us

profile of v9, /device:TPU:1, one launch (start us, length us, event | category | flops | bytes accessed | tf_op | source)
XLA Modules:
  0.0 132.4 jit_solution(8200314734191877542)
XLA Ops:
  0.6 126.6 %whole.1 = (bf16[2,224,2048]{2,1,0:T(8,128)(2,1)}, bf16[2,224,2048]{2,1,0:T(8,128)(2,1)}, bf16[2,224,2048]{2,1,0:T(8,128)(2,1)}, bf16[64,512]{1,0:T(8,128)(2,1)}) custom-call(f32[4,2,64,1792]{3,2,1,0:T(8,128)} %bitcast.11, f32[4,2,64,1792]{3,2,1,0:T(8,128)} %bitcast.12, f32[4,2,64,1792]{3,2,1,0:T(8,128)} %bitcast.13, f32[1,64]{1,0:T(1,128)} %bitcast.17, ...), custom_call_target="tpu_custom_call" | custom-call | tf_op jit(solution)/shard_map/whole/pallas_call | solution.py:538
  127.2 5.1 %deliver.1 = (bf16[2,224,2048]{2,1,0:T(8,128)(2,1)}, bf16[2,224,2048]{2,1,0:T(8,128)(2,1)}, bf16[2,224,2048]{2,1,0:T(8,128)(2,1)}, bf16[64,512]{1,0:T(8,128)(2,1)}) custom-call(bf16[2,224,2048]{2,1,0:T(8,128)(2,1)} %get-tuple-element.12.refs_0_, bf16[2,224,2048]{2,1,0:T(8,128)(2,1)} %get-tuple-element.13.refs_1_, ...), custom_call_target="tpu_custom_call" | custom-call | tf_op jit(solution)/shard_map/deliver/pallas_call | solution.py:599

commit v10 on v9

--- a/solution.py
+++ b/solution.py
@@ -120,10 +120,13 @@
 
     def gather(l, s):
         axis = ROUTES[l][2][s]
-        flows["g", l, s] = [
-            start(push(part(l, s), part(l, s), gs.at[l, s, i], gr.at[l, s, i], {axis: along(axis, h)}))
-            for i, h in enumerate(HOPS)
-        ]
+        for h in HOPS:
+            push(part(l, s), part(l, s), gs.at[l, s], gr.at[l, s], {axis: along(axis, h)}).start()
+        rows = pl.ds(0, ROUTES[l][1])
+        three = tokens.at[0, 0:3, :, 0, rows] if s else tokens.at[0, 0, 0:3, 0, rows]
+        all_three = bulk(three, gs.at[l, s], gr.at[l, s])
+        sends.append(all_three)
+        flows["g", l, s] = [all_three]
 
     for l in range(3):
         gather(l, 0)
@@ -557,7 +560,7 @@
         + [dma, dma((len(PARTS),)), dma, dma((len(PARTS),)), dma((2,)), dma((len(PARTS),))]
         + [dma] * 4
         + [dma((3,))] * 2
-        + [dma((3, 2, 3))] * 2
+        + [dma((3, 2))] * 2
         + [dma((3, 4))] * 2
         + [dma((6,))] * 2
         + [dma((3,))]

time: 133 us -> 132 us (level)
  no operation moved by 1% of the time
where the time goes in v10:
time: 132 us
  Pallas kernels  131 us (99%)
    pallas_call x1, Pallas kernels, whole_call(): pl.pallas_call(whole, out_shape=(served, served, served, jax.ShapeDtypeSt...  126 us
    pallas_call x1, Pallas kernels, deliver_call(): pl.pallas_call(deliver, out_shape=tuple((jax.ShapeDtypeStruct(r.shape, r....  5.05 us

profile of v10, /device:TPU:1, one launch (start us, length us, event | category | flops | bytes accessed | tf_op | source)
XLA Modules:
  0.0 132.2 jit_solution(17935282435107459187)
XLA Ops:
  0.6 126.4 %whole.1 = (bf16[2,224,2048]{2,1,0:T(8,128)(2,1)}, bf16[2,224,2048]{2,1,0:T(8,128)(2,1)}, bf16[2,224,2048]{2,1,0:T(8,128)(2,1)}, bf16[64,512]{1,0:T(8,128)(2,1)}) custom-call(f32[4,2,64,1792]{3,2,1,0:T(8,128)} %bitcast.11, f32[4,2,64,1792]{3,2,1,0:T(8,128)} %bitcast.12, f32[4,2,64,1792]{3,2,1,0:T(8,128)} %bitcast.13, f32[1,64]{1,0:T(1,128)} %bitcast.17, ...), custom_call_target="tpu_custom_call" | custom-call | tf_op jit(solution)/shard_map/whole/pallas_call | solution.py:541
  127.0 5.1 %deliver.1 = (bf16[2,224,2048]{2,1,0:T(8,128)(2,1)}, bf16[2,224,2048]{2,1,0:T(8,128)(2,1)}, bf16[2,224,2048]{2,1,0:T(8,128)(2,1)}, bf16[64,512]{1,0:T(8,128)(2,1)}) custom-call(bf16[2,224,2048]{2,1,0:T(8,128)(2,1)} %get-tuple-element.12.refs_0_, bf16[2,224,2048]{2,1,0:T(8,128)(2,1)} %get-tuple-element.13.refs_1_, ...), custom_call_target="tpu_custom_call" | custom-call | tf_op jit(solution)/shard_map/deliver/pallas_call | solution.py:602
